TPU v7x, 512 devices: a whole 4x8x8 slice. The times are simulated.
512 devices in a mesh: sp: 128 (over z, y, core), tp: 4 (over x).
Axes of the slice: x: 4, y: 8, z: 8, core: 2. Of those that a mesh axis runs over, the one named last changes fastest.
Arguments:
- tokens: bfloat16 [24576, 2048], P('sp'), may hold values from -6 to 6
- norm_gain: float32 [2048], replicated, may hold values from 0.1 to 1.9
- conv_value_w: bfloat16 [2048, 1024], P('sp', 'tp'), may hold values from -0.125 to 0.125
- conv_gate_w: bfloat16 [2048, 1024], P('sp', 'tp'), may hold values from -0.125 to 0.125
- query_w: bfloat16 [2048, 1024], P('sp', 'tp'), may hold values from -0.125 to 0.125
- key_w: bfloat16 [2048, 1024], P('sp', 'tp'), may hold values from -0.125 to 0.125
- value_w: bfloat16 [2048, 1024], P('sp', 'tp'), may hold values from -0.125 to 0.125
- out_gate_w: bfloat16 [2048, 1024], P('sp', 'tp'), may hold values from -0.125 to 0.125
- conv_out_w: bfloat16 [2048, 1024], P('sp', 'tp'), may hold values from -0.125 to 0.125
- ret_out_w: bfloat16 [2048, 1024], P('sp', 'tp'), may hold values from -0.125 to 0.125
- conv_taps: bfloat16 [31, 1024], replicated, may hold values from -3 to 3
- conv_gain: float32 [1024], replicated, may hold values from 0.1 to 1.9
- ret_gain: float32 [1024], replicated, may hold values from 0.1 to 1.9
- log_decay: float32 [8, 24576], P('tp', 'sp'), may hold values from -1 to 0, as said below
Outputs:
- mixed: bfloat16 [24576, 2048], P(('sp', 'tp'))
Inputs may be any that keep to these rules, and one draw needn't show every extreme that they name: `log_decay`: every entry is at most zero.
All inputs are finite; a program needn't handle non-finite values.
Results may differ from a plain program's by a relative error of at most 0.03.
Values may be sent and summed in bfloat16 or wider, within the bound.
No kernel may reach another device: no remote copies, remote signals or barrier semaphores. Data moves between devices by JAX's collectives and lax.ppermute only.
A program may use at most 64 MiB of HBM per device.

v0:
```python
import jax
import jax.numpy as jnp
from jax import lax
from jax.experimental import pallas as pl
from jax.experimental.pallas import tpu as pltpu
from jax.sharding import Mesh
from jax.sharding import PartitionSpec as P


CONV_DIM = 1024
HEAD_DIM = 128
CONV_WIDTH = 31
HALO = 32
SP = ("sp_0", "sp_1", "sp_2")
SP_TP = ("sp_0", "sp_1", "sp_2", "tp")
EPSILON = 1e-06
ROPE_BASE = 10000.0
RING = 8
KV_MIB = 14
KV_FAR = ()
BF = jnp.bfloat16
F32 = jnp.float32


def place(z, y, core):
    return (z * RING + y) * 2 + core


def ring_groups(first):
    along_y = [[place(z, y, 0 if first else 1) for y in range(RING)] for z in range(RING)]
    along_z = [[place(z, y, 1 if first else 0) for z in range(RING)] for y in range(RING)]
    return along_y + along_z


def told_to_all(x, axis, groups=None, count=RING):
    copies = jnp.broadcast_to(x[None], (count, *x.shape))
    return lax.all_to_all(copies, axis, 0, 0, axis_index_groups=groups, tiled=True)


def call(body, outs, scalars, arrays, scratch=(), far=(), parts=(), far_outs=(), mib=56):
    n, m = len(arrays), len(outs)
    near = [pltpu.VMEM(arrays[i].shape, arrays[i].dtype) for i in far]
    near += [pltpu.VMEM((RING, 256, 256), BF) for _ in parts]
    near += [pltpu.VMEM(outs[i].shape, outs[i].dtype) for i in far_outs]
    scratch = list(scratch)

    def whole(where_ref, *refs):
        ins, rest = list(refs[:n]), refs[n:]
        results, rest = rest[:m], rest[m:]
        own, rest = rest[: len(scratch)], rest[len(scratch) :]
        results, sem = list(results), rest[-1] if near else None
        sources = [ins[i] for i in far] + [ins[i].at[:, p] for i, p in parts]
        copies = [pltpu.make_async_copy(a, rest[k], sem.at[k]) for k, a in enumerate(sources)]
        for c in copies:
            c.start()
        for c in copies:
            c.wait()
        for k, i in enumerate([*far, *(i for i, _ in parts)]):
            ins[i] = rest[k]
        copies = []
        for k, i in enumerate(far_outs, len(sources)):
            copies.append(pltpu.make_async_copy(rest[k], results[i], sem.at[k]))
            results[i] = rest[k]
        body(where_ref, *ins, *results, *own)
        for c in copies:
            c.start()
        for c in copies:
            c.wait()

    def spec(is_far):
        return pl.BlockSpec(memory_space=pltpu.HBM if is_far else pltpu.VMEM)

    sems = [pltpu.SemaphoreType.DMA((len(near),))] if near else []
    return pl.pallas_call(
        whole,
        out_shape=outs,
        in_specs=[pl.BlockSpec(memory_space=pltpu.SMEM)] + [spec(i in far or i in [j for j, _ in parts]) for i in range(n)],
        out_specs=[spec(i in far_outs) for i in range(m)],
        scratch_shapes=scratch + near + sems,
        compiler_params=pltpu.CompilerParams(vmem_limit_bytes=mib * 1024 * 1024),
    )(scalars, *arrays)


def like(shape, kind):
    return jax.ShapeDtypeStruct(shape, kind)


def tall_dot(a, b, contract):
    return lax.dot_general(a, b, (contract, ((), ())), precision=lax.Precision.HIGHEST, preferred_element_type=F32)


def scaled(x, gain):
    wide = x.astype(F32)
    mean = jnp.mean(wide * wide, axis=-1, keepdims=True)
    return (wide * lax.rsqrt(mean + EPSILON) * gain).astype(BF)


def prepare(where_ref, own_ref, partner_ref, gain_ref, normed_ref):
    core = where_ref[2]
    gain = gain_ref[...]
    rows = own_ref.shape[0]
    for k in range(rows // 64):
        at = pl.multiple_of(core * rows + k * 64, 32)
        normed_ref[pl.ds(at, 64), :] = scaled(own_ref[k * 64 : (k + 1) * 64, :], gain)
        at = pl.multiple_of((1 - core) * rows + k * 64, 32)
        normed_ref[pl.ds(at, 64), :] = scaled(partner_ref[k * 64 : (k + 1) * 64, :], gain)


def decays(where_ref, log_ref, other_log_ref, col_ref, row_ref):
    core = where_ref[2]
    rows = log_ref.shape[1]
    own = jnp.where(core == 0, log_ref[0:1, :], log_ref[1:2, :])
    other = other_log_ref[...]
    upto = lax.broadcasted_iota(jnp.int32, (rows, rows), 0) >= lax.broadcasted_iota(jnp.int32, (rows, rows), 1)
    upto = jnp.where(upto, 1.0, 0.0)

    def summed(x):
        return tall_dot(upto, jnp.broadcast_to(x, (HEAD_DIM, rows)), ((1,), (1,)))

    first = summed(jnp.where(core == 0, own, other))
    second = summed(jnp.where(core == 0, other, own)) + first[rows - 1 : rows, :]
    col_ref[0:rows, :] = first
    col_ref[rows:, :] = second
    pick = jnp.where(lax.broadcasted_iota(jnp.int32, (8, HEAD_DIM), 1) == 0, 1.0, 0.0)
    row_ref[...] = tall_dot(pick, col_ref[...], ((1,), (1,)))


def spread(mine_ref, theirs_ref, out_ref):
    core = lax.axis_index("sp_2")
    height = mine_ref.shape[0]
    at = pl.multiple_of(core * height, 16)
    other = pl.multiple_of((1 - core) * height, 16)
    mine, theirs = mine_ref[...], theirs_ref[...]
    for k in range(RING):
        out_ref[k, pl.ds(at, height), :] = mine
        out_ref[k, pl.ds(other, height), :] = theirs


def assemble(*refs):
    weights, (mine_ref, other_ref, sem) = refs[:8], refs[8:]
    core = lax.axis_index("sp_2")
    copies = []
    for h, out_ref in ((core, mine_ref), (1 - core, other_ref)):
        at = pl.multiple_of(h * HEAD_DIM, HEAD_DIM)
        for k, w_ref in enumerate(weights):
            target = out_ref.at[:, k * HEAD_DIM : (k + 1) * HEAD_DIM]
            copies.append(pltpu.make_async_copy(w_ref.at[:, pl.ds(at, HEAD_DIM)], target, sem.at[len(copies)]))
    for c in copies:
        c.start()
    for c in copies:
        c.wait()


def set_rows(target_ref, core, block, rows, first=0):
    height = rows.shape[0]

    @pl.when(core == 0)
    def _():
        target_ref[pl.ds(pl.multiple_of(block * 256 + first, 32), height), :] = rows

    @pl.when(core == 1)
    def _():
        for k in range(height // 32):
            at = pl.multiple_of((first // 32 + k) * 256 + block * 32, 32)
            target_ref[pl.ds(at, 32), :] = rows[k * 32 : (k + 1) * 32, :]


def rotated(raw, cosine, sine):
    half = pltpu.roll(raw, HEAD_DIM // 2, 1)
    return raw * cosine + half * sine


def key_value(where_ref, normed_ref, blocks_ref, cos_ref, sin_ref, col_ref, both_ref, sent_ref, w_ref):
    core = where_ref[2]
    for k in range(RING):
        set_rows(w_ref, core, k, blocks_ref[k])
    both = jnp.dot(normed_ref[...], w_ref[...], preferred_element_type=F32)
    raw = both[:, :HEAD_DIM].astype(BF).astype(F32)
    value = both[:, HEAD_DIM:].astype(BF)
    key = rotated(raw, cos_ref[...], sin_ref[...]).astype(BF)
    both_ref[:, :HEAD_DIM] = key
    both_ref[:, HEAD_DIM:] = value
    rows = key.shape[0]
    total = col_ref[rows - 1 : rows, :]
    weighted = (key.astype(F32) * jnp.exp(total - col_ref[...])).astype(BF)
    state = lax.dot_general(weighted, value, (((0,), (0,)), ((), ())), preferred_element_type=F32)
    send_state(sent_ref, state, total)


def send_state(sent_ref, state, log):
    high, middle, low = in_parts(log)
    row = lax.broadcasted_iota(jnp.int32, (16, HEAD_DIM), 0)
    logs = jnp.where(row == 0, high.astype(F32), jnp.where(row == 1, middle.astype(F32), jnp.where(row == 2, low.astype(F32), 0.0)))
    state, logs = state.astype(BF), logs.astype(BF)
    for k in range(RING):
        sent_ref[k, 0:HEAD_DIM, :] = state
        sent_ref[k, HEAD_DIM : HEAD_DIM + 16, :] = logs


def in_order(target_ref, core, near_ref):
    for k in range(RING):
        set_rows(target_ref, core, k, near_ref[k])


def log_of(ref, k):
    parts = ref[k, HEAD_DIM : HEAD_DIM + 16, :].astype(F32)
    return parts[0:1] + parts[1:2] + parts[2:3]


def in_parts(x):
    high = x.astype(BF)
    rest = x - high.astype(F32)
    middle = rest.astype(BF)
    low = (rest - middle.astype(F32)).astype(BF)
    return high, middle, low


def along_row(where_ref, got_ref, inside_ref, sent_ref):
    here = where_ref[1]
    before = jnp.zeros((1, HEAD_DIM), F32)
    whole = jnp.zeros((1, HEAD_DIM), F32)
    inside = jnp.zeros((HEAD_DIM, HEAD_DIM), F32)
    total = jnp.zeros((HEAD_DIM, HEAD_DIM), F32)
    for k in reversed(range(RING)):
        log = log_of(got_ref, k)
        state = got_ref[k, 0:HEAD_DIM, :].astype(F32)
        inside = inside + jnp.where(k < here, jnp.exp(before), 0.0) * state
        total = total + jnp.exp(whole) * state
        before = before + jnp.where(k < here, log, 0.0)
        whole = whole + log
    inside_ref[0:HEAD_DIM, :] = inside
    inside_ref[HEAD_DIM:, :] = jnp.broadcast_to(jnp.exp(before), (8, HEAD_DIM))
    send_state(sent_ref, total, whole)


def conv_part(where_ref, normed_ref, halo_ref, gain_ref, taps_ref, near_ref, sums_ref, stats_ref, w_ref, gated_ref):
    channel = pl.multiple_of((where_ref[3] * 2 + where_ref[2]) * HEAD_DIM, HEAD_DIM)
    in_order(w_ref, where_ref[2], near_ref)

    def gated(x):
        both = jnp.dot(x, w_ref[...], preferred_element_type=F32)
        value = both[:, :HEAD_DIM].astype(BF).astype(F32)
        gate = both[:, HEAD_DIM:].astype(BF).astype(F32)
        return (value * jax.nn.sigmoid(gate)).astype(BF).astype(F32)

    gated_ref[0:HALO, :] = gated(scaled(halo_ref[...], gain_ref[...]))
    gated_ref[HALO:, :] = gated(normed_ref[...])
    taps = taps_ref[:, pl.ds(channel, HEAD_DIM)].astype(F32)
    rows = sums_ref.shape[0]
    lead = HALO - CONV_WIDTH + 1
    for at in range(0, rows, 64):
        total = jnp.zeros((64, HEAD_DIM), F32)
        for w in range(CONV_WIDTH):
            total = total + gated_ref[at + lead + w : at + lead + w + 64, :] * taps[w : w + 1, :]
        sums_ref[at : at + 64, :] = total
    sums = sums_ref[...]
    ones = jnp.ones((8, HEAD_DIM), F32)
    over_lanes = (((1,), (1,)), ((), ()))
    first = lax.dot_general(ones, sums, over_lanes, precision=lax.Precision.HIGHEST, preferred_element_type=F32)
    second = lax.dot_general(ones, sums * sums, over_lanes, precision=lax.Precision.HIGHEST, preferred_element_type=F32)
    for k in range(8):
        stats_ref[k, 0:1, :] = first[0:1]
        stats_ref[k, 1:2, :] = second[0:1]


def inner_part(where_ref, normed_ref, cos_ref, sin_ref, key_value_ref, col_ref, row_ref, sums_ref, near_ref, packed_ref, qg_ref):
    in_order(qg_ref, where_ref[2], near_ref)
    both = jnp.dot(normed_ref[...], qg_ref[...], preferred_element_type=F32)
    raw = both[:, :HEAD_DIM].astype(BF).astype(F32)
    gate = both[:, HEAD_DIM:].astype(BF).astype(F32)
    query = (rotated(raw, cos_ref[...], sin_ref[...]) * HEAD_DIM ** (-0.5)).astype(BF)
    packed_ref[:, HEAD_DIM : 2 * HEAD_DIM] = query.astype(F32)
    packed_ref[:, 2 * HEAD_DIM : 3 * HEAD_DIM] = gate * jax.nn.sigmoid(gate)
    packed_ref[:, 3 * HEAD_DIM : 4 * HEAD_DIM] = jnp.exp(col_ref[...])
    packed_ref[:, 4 * HEAD_DIM :] = sums_ref[...]
    rows = query.shape[0]
    for at in range(0, rows, 128):
        upto = at + 128
        scores = lax.dot_general(query[at:upto], key_value_ref[0:upto, :HEAD_DIM], (((1,), (1,)), ((), ())), preferred_element_type=F32)
        mine = lax.broadcasted_iota(jnp.int32, scores.shape, 0) + at
        other = lax.broadcasted_iota(jnp.int32, scores.shape, 1)
        seen = mine >= other
        gap = col_ref[at:upto, 0:1] - row_ref[0:1, 0:upto]
        decay = jnp.where(seen, jnp.exp(jnp.where(seen, gap, 0.0)), 0.0)
        weight = (scores * decay).astype(BF)
        packed_ref[at:upto, :HEAD_DIM] = jnp.dot(weight, key_value_ref[0:upto, HEAD_DIM:], preferred_element_type=F32)


def outer_part(where_ref, packed_ref, inside_ref, got_ref, gain_ref, stats_ref, conv_gain_ref, blocks_ref, keep_ref, send_ref, hidden_ref, out_ref):
    core = where_ref[2]
    here = where_ref[0]
    channel = pl.multiple_of((where_ref[3] * 2 + core) * HEAD_DIM, HEAD_DIM)
    before = jnp.zeros((1, HEAD_DIM), F32)
    rows_before = jnp.zeros((HEAD_DIM, HEAD_DIM), F32)
    for k in reversed(range(RING)):
        log = log_of(got_ref, k)
        state = got_ref[k, 0:HEAD_DIM, :].astype(F32)
        rows_before = rows_before + jnp.where(k < here, jnp.exp(before), 0.0) * state
        before = before + jnp.where(k < here, log, 0.0)
    state = inside_ref[0:HEAD_DIM, :] + inside_ref[HEAD_DIM : HEAD_DIM + 1, :] * rows_before
    cross = jnp.dot(packed_ref[:, HEAD_DIM : 2 * HEAD_DIM], state, preferred_element_type=F32)
    merged = packed_ref[:, :HEAD_DIM] + cross * packed_ref[:, 3 * HEAD_DIM : 4 * HEAD_DIM]
    centred = merged - jnp.mean(merged, axis=-1, keepdims=True)
    spread = jnp.mean(centred * centred, axis=-1, keepdims=True)
    normed = centred * lax.rsqrt(spread + EPSILON) * gain_ref[:, pl.ds(channel, HEAD_DIM)]
    hidden_ref[:, HEAD_DIM:] = (packed_ref[:, 2 * HEAD_DIM : 3 * HEAD_DIM] * normed).astype(BF)
    ones = jnp.ones((8, HEAD_DIM), F32)
    over_peers = (((0,), (0,)), ((), ()))
    firsts = jnp.concatenate([stats_ref[k, 0:1, :] for k in range(8)], axis=0)
    seconds = jnp.concatenate([stats_ref[k, 1:2, :] for k in range(8)], axis=0)
    mean = lax.dot_general(firsts, ones, over_peers, precision=lax.Precision.HIGHEST, preferred_element_type=F32) / CONV_DIM
    square = lax.dot_general(seconds, ones, over_peers, precision=lax.Precision.HIGHEST, preferred_element_type=F32) / CONV_DIM
    chan_var = square - mean * mean
    v = (packed_ref[:, 4 * HEAD_DIM :] - mean) * lax.rsqrt(chan_var + EPSILON) * conv_gain_ref[:, pl.ds(channel, HEAD_DIM)]
    hidden_ref[:, :HEAD_DIM] = (v * jax.nn.sigmoid(v)).astype(BF)
    half = keep_ref.shape[0]
    for k in range(RING):
        set_rows(out_ref, core, k, blocks_ref[k, 2])
    mine = hidden_ref[pl.ds(pl.multiple_of(core * half, 64), half), :]
    theirs = hidden_ref[pl.ds(pl.multiple_of((1 - core) * half, 64), half), :]
    over_channels = (((1,), (1,)), ((), ()))
    send_ref[...] = lax.dot_general(theirs, out_ref[...], over_channels, preferred_element_type=F32).astype(BF)
    keep_ref[...] = lax.dot_general(mine, out_ref[...], over_channels, preferred_element_type=F32).astype(BF)


def rotary_tables(start, count):
    half = HEAD_DIM // 2
    frequency = ROPE_BASE ** (-jnp.arange(0, HEAD_DIM, 2, dtype=F32) / HEAD_DIM)
    positions = start + jnp.arange(count, dtype=jnp.int32)
    angles = positions.astype(F32)[:, None] * frequency[None, :]
    cosine, sine = jnp.cos(angles), jnp.sin(angles)
    del half
    return jnp.concatenate([cosine, cosine], axis=1), jnp.concatenate([-sine, sine], axis=1)


def per_device(
    tokens,
    norm_gain,
    conv_value_w,
    conv_gate_w,
    query_w,
    key_w,
    value_w,
    out_gate_w,
    conv_out_w,
    ret_out_w,
    conv_taps,
    conv_gain,
    ret_gain,
    log_decay,
):
    rows, width = tokens.shape
    both_rows = 2 * rows
    z, y, core, x = (lax.axis_index(a) for a in SP_TP)
    chip = z * RING + y
    where = jnp.stack([z, y, core, x]).astype(jnp.int32)

    parts = (key_w, value_w, conv_value_w, conv_gate_w, query_w, out_gate_w, conv_out_w, ret_out_w)
    half = like((key_w.shape[0], 8 * HEAD_DIM), BF)
    mine, other = pl.pallas_call(
        assemble,
        out_shape=[half, half],
        in_specs=[pl.BlockSpec(memory_space=pl.ANY) for _ in parts],
        out_specs=[pl.BlockSpec(memory_space=pltpu.VMEM)] * 2,
        scratch_shapes=[pltpu.SemaphoreType.DMA((16,))],
        compiler_params=pltpu.CompilerParams(vmem_limit_bytes=56 * 1024 * 1024),
        name="assemble",
    )(*parts)
    swap = [(0, 1), (1, 0)]
    theirs = lax.ppermute(other, "sp_2", swap)
    copies = pl.pallas_call(
        spread,
        out_shape=like((RING, 2 * key_w.shape[0], 8 * HEAD_DIM), BF),
        in_specs=[pl.BlockSpec(memory_space=pltpu.VMEM)] * 2,
        out_specs=pl.BlockSpec(memory_space=pltpu.VMEM),
        compiler_params=pltpu.CompilerParams(vmem_limit_bytes=4 * 1024 * 1024),
        name="spread",
    )(mine, theirs)
    stage = lax.all_to_all(copies, SP, 0, 0, axis_index_groups=ring_groups(True), tiled=True)
    stage = stage.reshape(-1, 8 * HEAD_DIM)

    partner = lax.ppermute(tokens, "sp_2", swap)
    other_log = lax.ppermute(lax.dynamic_slice_in_dim(log_decay, 1 - core, 1, 0), "sp_2", swap)
    (normed,) = call(
        prepare, [like((both_rows, width), BF)], where, (tokens, partner, norm_gain.reshape(1, width)), far=(0, 1)
    )
    stage, other_log, normed = lax.optimization_barrier((stage, other_log, normed))
    col, row = call(
        decays, [like((both_rows, HEAD_DIM), F32), like((8, both_rows), F32)], where, (log_decay, other_log), mib=8
    )
    cosine, sine = rotary_tables(chip * both_rows, both_rows)

    first = told_to_all(stage[:, : 2 * HEAD_DIM], SP, ring_groups(False))
    others = jnp.moveaxis(stage[:, 2 * HEAD_DIM :].reshape(-1, 3, 2 * HEAD_DIM), 1, 0)[None]
    others, col = lax.optimization_barrier((others, col))
    others = lax.all_gather(others, SP, axis=0, axis_index_groups=ring_groups(False), tiled=True)

    key_value_rows, sent = call(
        key_value,
        [like((both_rows, 2 * HEAD_DIM), BF), like((RING, HEAD_DIM + 16, HEAD_DIM), BF)],
        where,
        (normed, first, cosine, sine, col),
        [pltpu.VMEM((width, 2 * HEAD_DIM), BF)],
        mib=KV_MIB,
        far=KV_FAR,
    )
    last = jnp.where(core == 1, tokens[rows - HALO :], partner[rows - HALO :])
    last, _ = lax.optimization_barrier((last, sent))
    onward = [(k * 2 + c, (k + 1) * 2 + c) for k in range(RING * RING - 1) for c in range(2)]
    halo = lax.ppermute(last, SP, onward)
    got = lax.all_to_all(sent, "sp_1", 0, 0, tiled=True)
    got, halo = lax.optimization_barrier((got, halo))
    inside, sent = call(
        along_row,
        [like((HEAD_DIM + 8, HEAD_DIM), F32), like((RING, HEAD_DIM + 16, HEAD_DIM), BF)],
        where,
        (got,),
        mib=14,
    )
    got = lax.all_to_all(sent, "sp_0", 0, 0, tiled=True)

    sums, stats = call(
        conv_part,
        [like((both_rows, HEAD_DIM), F32), like((8, 2, both_rows), F32)],
        where,
        (normed, halo, norm_gain.reshape(1, width), conv_taps, others),
        [pltpu.VMEM((width, 2 * HEAD_DIM), BF), pltpu.VMEM((HALO + both_rows, HEAD_DIM), F32)],
        far=(0, 1, 2),
        parts=((4, 0),),
        far_outs=(0, 1),
    )
    (packed,) = call(
        inner_part,
        [like((both_rows, 5 * HEAD_DIM), F32)],
        where,
        (normed, cosine, sine, key_value_rows, col, row, sums, others),
        [pltpu.VMEM((width, 2 * HEAD_DIM), BF)],
        far=(0, 1, 2, 3, 4, 5, 6),
        parts=((7, 1),),
        far_outs=(0,),
    )
    stats, packed, got = lax.optimization_barrier((stats, packed, got))
    stats = lax.all_to_all(stats, ("sp_2", "tp"), 0, 0, tiled=True)
    keep, send = call(
        outer_part,
        [like((rows, width), BF), like((rows, width), BF)],
        where,
        (packed, inside, got, ret_gain.reshape(1, -1), stats, conv_gain.reshape(1, -1), others),
        [pltpu.VMEM((both_rows, 2 * HEAD_DIM), BF), pltpu.VMEM((width, 2 * HEAD_DIM), BF)],
        mib=14,
    )
    other = lax.ppermute(send, "sp_2", swap)
    partial = (keep.astype(F32) + other.astype(F32)).astype(BF)
    peers = lax.axis_size("tp")
    arrived = lax.all_to_all(partial.reshape(peers, rows // peers, width), "tp", 0, 0, tiled=True)
    return arrived.astype(F32).sum(axis=0).astype(BF)


def solution(mesh):
    finer = Mesh(mesh.devices.reshape(8, 8, 2, mesh.shape["tp"]), SP_TP)
    weight = P(SP, "tp")
    return jax.shard_map(
        per_device,
        mesh=finer,
        in_specs=(P(SP, None), P(), *[weight] * 8, P(), P(), P(), P("tp", SP)),
        out_specs=P(SP_TP, None),
        check_vma=False,
    )
```

profile of v0, /device:TPU:1, one launch (start us, length us, event | category | flops | bytes accessed | tf_op | source)
XLA Modules:
  0.0 146.4 jit_solution(4400990977935538476)
XLA Ops:
  6.5 1.6 %assemble.1 = (bf16[16,1024]{1,0:T(8,128)(2,1)}, bf16[16,1024]{1,0:T(8,128)(2,1)}) custom-call(bf16[16,256]{1,0:T(8,128)(2,1)} %refs_0_.3, bf16[16,256]{1,0:T(8,128)(2,1)} %refs_1_.1, bf16[16,256]{1,0:T(8,128)(2,1)} %refs_2_.1, bf16[16,256]{1,0:T(8,128)(2,1)} %refs_3_.2, bf16[16,256]{1,0:T(8,128)(2,1)} %refs_4_.1, bf16[16,256]{1,0:T(8,128)(2,1)} %refs_5_.1, ...), custom_call_target="tpu_custom_call" | custom-call | tf_op jit(solution)/shard_map/assemble/pallas_call | solution.py:360
  8.1 8.7 %collective-permute-start = (bf16[16,1024]{1,0:T(8,128)(2,1)}, bf16[16,1024]{1,0:T(8,128)(2,1)S(1)}, u32[]{:S(2)}, u32[]{:S(2)}) collective-permute-start(bf16[16,1024]{1,0:T(8,128)(2,1)} %get-tuple-element.29), channel_id=1, source_target_pairs={{0,4},{4,0},{1,5},{5,1},{2,6},{6,2},{3,7},{7,3},{8,12},{12,8},{9,1... | collective-permute-start | bytes 98312 | tf_op jit(solution)/shard_map/ppermute | solution.py:370
  16.9 1.0 collective-permute-done.theirs_ref
  18.0 0.8 copy-done.7
  18.7 0.8 spread.1
  19.5 4.7 %all-to-all-start = ((bf16[8,32,1024]{2,1,0:T(8,128)(2,1)}), bf16[8,32,1024]{2,1,0:T(8,128)(2,1)S(1)}, u32[]{:S(2)}, u32[]{:S(2)}) async-start(bf16[8,32,1024]{2,1,0:T(8,128)(2,1)} %spread.1), calls=%async_computation | async-start | bytes 1048576 | tf_op jit(solution)/shard_map/all_to_all | solution.py:379
  24.2 0.0 all-gather.2.cloned.1.call-start
  24.3 0.0 copy-done.14
  24.3 1.9 %collective-permute-start.2 = (bf16[192,2048]{1,0:T(8,128)(2,1)S(1)}, bf16[192,2048]{1,0:T(8,128)(2,1)}, u32[]{:S(2)}, u32[]{:S(2)}) collective-permute-start(bf16[192,2048]{1,0:T(8,128)(2,1)S(1)} %copy-done.14), channel_id=1, source_target_pairs={{0,4},{4,0},{1,5},{5,1},{2,6},{6,2},{3,7},{7,3},{8,12},{12,8},{9,1... | collective-permute-start | bytes 2359304 | tf_op jit(solution)/shard_map/ppermute | solution.py:382
  26.2 0.0 copy-done.11
  26.2 2.4 %collective-permute-start.1 = (f32[1,192]{1,0:T(1,128)S(1)}, f32[1,192]{1,0:T(1,128)S(1)}, u32[]{:S(2)}, u32[]{:S(2)}) collective-permute-start(f32[1,192]{1,0:T(1,128)S(1)} %constant_dynamic-slice_fusion), channel_id=1, source_target_pairs={{0,4},{4,0},{1,5},{5,1},{2,6},{6,2},{3,7},{7,3},{8,12},{12,8},{9,1... | collective-permute-start | bytes 2312 | tf_op jit(solution)/shard_map/ppermute | solution.py:383
  28.7 0.6 pad_add_fusion.where_ref
  29.2 0.0 collective-permute-done.2.refs_1_
  29.3 3.8 %shard_map.136.refs_0_ = bf16[384,2048]{1,0:T(8,128)(2,1)} custom-call(s32[4]{0:T(128)} %pad_add_fusion.where_ref, bf16[192,2048]{1,0:T(8,128)(2,1)} %refs_0_.4, bf16[192,2048]{1,0:T(8,128)(2,1)} %collective-permute-done.2.refs_1_, f32[1,2048]{1,0:T(1,128)} %bitcast.20), custom_call_target="tpu_custom_call" | custom-call | tf_op jit(solution)/shard_map/pallas_call | solution.py:74
  33.1 0.0 copy-start.8
  33.1 0.0 collective-permute-done.1.refs_1_
  33.1 3.3 %all-to-all-done = bf16[8,32,1024]{2,1,0:T(8,128)(2,1)S(1)} async-done(((bf16[8,32,1024]{2,1,0:T(8,128)(2,1)}), bf16[8,32,1024]{2,1,0:T(8,128)(2,1)S(1)}, u32[]{:S(2)}, u32[]{:S(2)}) %all-to-all-start) | async-done | bytes 524320 | tf_op jit(solution)/shard_map/all_to_all | solution.py:379
  36.4 0.2 copy.17
  36.6 0.0 copy-done.8
  36.6 1.3 shard_map.137
  38.0 1.0 copy.18
  38.9 0.0 all-gather.2.cloned.1.call-update
  39.0 1.0 broadcast_in_dim.4
  40.0 0.0 copy-done.10
  40.0 7.0 %all-to-all-start.1 = ((bf16[8,256,256]{2,1,0:T(8,128)(2,1)}), bf16[8,256,256]{2,1,0:T(8,128)(2,1)S(1)}, u32[]{:S(2)}, u32[]{:S(2)}) async-start(bf16[8,256,256]{2,1,0:T(8,128)(2,1)} %broadcast_in_dim.4), calls=%async_computation.1 | async-start | bytes 2097152 | tf_op jit(solution)/shard_map/all_to_all | solution.py:37
  47.0 0.8 fusion
  47.8 0.2 pad_maximum_fusion
  47.9 0.0 copy-start.3
  48.0 0.0 copy-start.4
  48.0 21.4 %all-to-all-done.1.refs_1_ = bf16[8,256,256]{2,1,0:T(8,128)(2,1)S(1)} async-done(((bf16[8,256,256]{2,1,0:T(8,128)(2,1)}), bf16[8,256,256]{2,1,0:T(8,128)(2,1)S(1)}, u32[]{:S(2)}, u32[]{:S(2)}) %all-to-all-start.1) | async-done | bytes 1048608 | tf_op jit(solution)/shard_map/all_to_all | solution.py:37
  69.4 0.0 copy-done.5
  69.4 0.0 copy-done.1
  69.4 2.3 %shard_map.138 = (bf16[384,256]{1,0:T(8,128)(2,1)S(1)}, bf16[8,144,128]{2,1,0:T(8,128)(2,1)}) custom-call(s32[4]{0:T(128)S(1)} %copy-done.8, bf16[384,2048]{1,0:T(8,128)(2,1)S(1)} %copy-done.1, bf16[8,256,256]{2,1,0:T(8,128)(2,1)S(1)} %all-to-all-done.1.refs_1_, f32[384,128]{1,0:T(8,128)S(1)} %get-tuple-element.54.refs_2_.refs_1_, ...), custom_call_target="tpu_custom_call" | custom-call | tf_op jit(solution)/shard_map/pallas_call | solution.py:74
  71.7 0.0 copy-done.3
  71.7 0.0 copy-done.4
  71.7 3.4 %all-to-all-start.2 = ((bf16[8,144,128]{2,1,0:T(8,128)(2,1)}), bf16[8,144,128]{2,1,0:T(8,128)(2,1)S(1)}, u32[]{:S(2)}, u32[]{:S(2)}) async-start(bf16[8,144,128]{2,1,0:T(8,128)(2,1)} %get-tuple-element.35), calls=%async_computation.2 | async-start | bytes 589824 | tf_op jit(solution)/shard_map/all_to_all | solution.py:411
  75.1 1.0 slice_select_fusion
  76.1 3.3 %collective-permute-start.3 = (bf16[32,2048]{1,0:T(8,128)(2,1)S(1)}, bf16[32,2048]{1,0:T(8,128)(2,1)S(1)}, u32[]{:S(2)}, u32[]{:S(2)}) collective-permute-start(bf16[32,2048]{1,0:T(8,128)(2,1)S(1)} %slice_select_fusion), channel_id=1, source_target_pairs={{0,8},{4,12},{8,16},{12,20},{16,24},{20,28},{24,32},{28,36},{32,40... | collective-permute-start | bytes 393224 | tf_op jit(solution)/shard_map/ppermute | solution.py:410
  79.4 5.8 %collective-permute-done.3.refs_1_ = bf16[32,2048]{1,0:T(8,128)(2,1)S(1)} collective-permute-done((bf16[32,2048]{1,0:T(8,128)(2,1)S(1)}, bf16[32,2048]{1,0:T(8,128)(2,1)S(1)}, u32[]{:S(2)}, u32[]{:S(2)}) %collective-permute-start.3) | collective-permute-done | bytes 131104 | tf_op jit(solution)/shard_map/ppermute | solution.py:410
  85.2 1.5 all-to-all-done.2.refs_0_
  86.6 1.3 shard_map.141
  88.0 5.8 %all-to-all-start.3 = ((bf16[8,144,128]{2,1,0:T(8,128)(2,1)}), bf16[8,144,128]{2,1,0:T(8,128)(2,1)S(1)}, u32[]{:S(2)}, u32[]{:S(2)}) async-start(bf16[8,144,128]{2,1,0:T(8,128)(2,1)} %get-tuple-element.44), calls=%async_computation.3 | async-start | bytes 589824 | tf_op jit(solution)/shard_map/all_to_all | solution.py:420
  93.8 0.0 all-gather.2.cloned.1.call-done.refs_4_.refs_7_.refs_6_
  93.8 0.0 copy-done.15
  93.8 5.4 %shard_map.139 = (f32[384,128]{1,0:T(8,128)}, f32[8,2,384]{2,1,0:T(2,128)}) custom-call(s32[4]{0:T(128)} %pad_add_fusion.where_ref, bf16[384,2048]{1,0:T(8,128)(2,1)} %shard_map.136.refs_0_, bf16[32,2048]{1,0:T(8,128)(2,1)} %copy-done.15, f32[1,2048]{1,0:T(1,128)} %bitcast.21, bf16[31,1024]{1,0:T(8,128)(2,1)} %refs_3_.3, ...), custom_call_target="tpu_custom_call" | custom-call | tf_op jit(solution)/shard_map/pallas_call | solution.py:74
  99.2 0.0 copy-done.6
  99.2 0.0 copy-start.16
  99.2 0.0 copy-start
  99.2 0.0 copy-start.9
  99.2 0.0 copy-start.12
  99.2 0.0 copy-start.13
  99.3 5.4 %shard_map.140.refs_0_ = f32[384,640]{1,0:T(8,128)} custom-call(s32[4]{0:T(128)} %pad_add_fusion.where_ref, bf16[384,2048]{1,0:T(8,128)(2,1)} %shard_map.136.refs_0_, f32[384,128]{1,0:T(8,128)} %copy-done.3, f32[384,128]{1,0:T(8,128)} %copy-done.4, bf16[384,256]{1,0:T(8,128)(2,1)} %copy-done.6, f32[384,128]{1,0:T(8,128)} %copy-done.5, f32[8,384]{1,0:T(8,128)} %copy-done.10, ...), custom_call_target="tpu_custom_call" | custom-call | tf_op jit(solution)/shard_map/pallas_call | solution.py:74
  104.7 0.0 all-to-all-done.3.refs_2_
  104.7 0.0 copy-done.16
  104.7 11.8 %all_to_all.30.refs_4_ = f32[8,2,384]{2,1,0:T(2,128)S(1)} all-to-all(f32[8,2,384]{2,1,0:T(2,128)S(1)} %copy-done.16), channel_id=1, replica_groups=mesh['sp_0'=8,'sp_1'=8,'sp_2'=2,'tp'=4] {'sp_2','tp'}, dimensions={0} | all-to-all | bytes 49152 | tf_op jit(solution)/shard_map/all_to_all | solution.py:443
  116.5 0.0 copy-done
  116.5 0.0 copy-done.9
  116.5 1.2 copy-done.2
  117.7 2.1 %shard_map.142 = (bf16[192,2048]{1,0:T(8,128)(2,1)S(1)}, bf16[192,2048]{1,0:T(8,128)(2,1)S(1)}) custom-call(s32[4]{0:T(128)S(1)} %copy-done.9, f32[384,640]{1,0:T(8,128)S(1)} %copy-done.2, f32[136,128]{1,0:T(8,128)S(1)} %get-tuple-element.46.refs_1_, bf16[8,144,128]{2,1,0:T(8,128)(2,1)S(1)} %all-to-all-done.3.refs_2_, f32[1,1024]{1,0:T(1,128)S(1)} %bitcast.14, ...), custom_call_target="tpu_custom_call" | custom-call | tf_op jit(solution)/shard_map/pallas_call | solution.py:74
  119.8 2.3 %collective-permute-start.4 = (bf16[192,2048]{1,0:T(8,128)(2,1)S(1)}, bf16[192,2048]{1,0:T(8,128)(2,1)S(1)}, u32[]{:S(2)}, u32[]{:S(2)}) collective-permute-start(bf16[192,2048]{1,0:T(8,128)(2,1)S(1)} %get-tuple-element.50), channel_id=1, source_target_pairs={{0,4},{4,0},{1,5},{5,1},{2,6},{6,2},{3,7},{7,3},{8,12},{12,8},{9,1... | collective-permute-start | bytes 2359304 | tf_op jit(solution)/shard_map/ppermute | solution.py:452
  122.1 1.9 %collective-permute-done.4 = bf16[192,2048]{1,0:T(8,128)(2,1)S(1)} collective-permute-done((bf16[192,2048]{1,0:T(8,128)(2,1)S(1)}, bf16[192,2048]{1,0:T(8,128)(2,1)S(1)}, u32[]{:S(2)}, u32[]{:S(2)}) %collective-permute-start.4) | collective-permute-done | bytes 786464 | tf_op jit(solution)/shard_map/ppermute | solution.py:452
  124.0 0.3 add_convert_fusion
  124.3 14.4 %all_to_all.31 = bf16[4,48,2048]{2,1,0:T(8,128)(2,1)S(1)} all-to-all(bf16[4,48,2048]{2,1,0:T(8,128)(2,1)S(1)} %bitcast.16), channel_id=1, replica_groups=mesh['sp_0'=8,'sp_1'=8,'sp_2'=2,'tp'=4] {'tp'}, dimensions={0} | all-to-all | bytes 1572864 | tf_op jit(solution)/shard_map/all_to_all | solution.py:455
  138.7 0.8 reduce_sum.12
  (16 shorter events, 0.1 us)
Async XLA Ops:
  6.5 19.7 %copy-start.11 = (f32[2,192]{1,0:T(2,128)S(1)}, f32[2,192]{1,0:T(2,128)}, u32[]{:S(2)}) copy-start(f32[2,192]{1,0:T(2,128)} %refs_0_.5) | copy-start | bytes 4612
  8.1 9.8 %collective-permute-start = (bf16[16,1024]{1,0:T(8,128)(2,1)}, bf16[16,1024]{1,0:T(8,128)(2,1)S(1)}, u32[]{:S(2)}, u32[]{:S(2)}) collective-permute-start(bf16[16,1024]{1,0:T(8,128)(2,1)} %get-tuple-element.29), channel_id=1, source_target_pairs={{0,4},{4,0},{1,5},{5,1},{2,6},{6,2},{3,7},{7,3},{8,12},{12,8},{9,1... | collective-permute-start | bytes 98312 | tf_op jit(solution)/shard_map/ppermute | solution.py:370
  18.0 0.8 copy-start.7
  18.7 5.6 %copy-start.14 = (bf16[192,2048]{1,0:T(8,128)(2,1)S(1)}, bf16[192,2048]{1,0:T(8,128)(2,1)}, u32[]{:S(2)}) copy-start(bf16[192,2048]{1,0:T(8,128)(2,1)} %refs_0_.4) | copy-start | bytes 2359300
  19.5 16.8 %all-to-all-start = ((bf16[8,32,1024]{2,1,0:T(8,128)(2,1)}), bf16[8,32,1024]{2,1,0:T(8,128)(2,1)S(1)}, u32[]{:S(2)}, u32[]{:S(2)}) async-start(bf16[8,32,1024]{2,1,0:T(8,128)(2,1)} %spread.1), calls=%async_computation | async-start | bytes 1048576 | tf_op jit(solution)/shard_map/all_to_all | solution.py:379
  24.2 69.6 %all-gather.2.cloned.1.call-start = ((), (), s32[]{:S(2)}) async-start(), calls=%async_computation.6 | async-start | bytes 3538944 | tf_op jit(solution)/shard_map/all_gather | solution.py:396
  24.3 5.0 %collective-permute-start.2 = (bf16[192,2048]{1,0:T(8,128)(2,1)S(1)}, bf16[192,2048]{1,0:T(8,128)(2,1)}, u32[]{:S(2)}, u32[]{:S(2)}) collective-permute-start(bf16[192,2048]{1,0:T(8,128)(2,1)S(1)} %copy-done.14), channel_id=1, source_target_pairs={{0,4},{4,0},{1,5},{5,1},{2,6},{6,2},{3,7},{7,3},{8,12},{12,8},{9,1... | collective-permute-start | bytes 2359304 | tf_op jit(solution)/shard_map/ppermute | solution.py:382
  26.2 6.9 %collective-permute-start.1 = (f32[1,192]{1,0:T(1,128)S(1)}, f32[1,192]{1,0:T(1,128)S(1)}, u32[]{:S(2)}, u32[]{:S(2)}) collective-permute-start(f32[1,192]{1,0:T(1,128)S(1)} %constant_dynamic-slice_fusion), channel_id=1, source_target_pairs={{0,4},{4,0},{1,5},{5,1},{2,6},{6,2},{3,7},{7,3},{8,12},{12,8},{9,1... | collective-permute-start | bytes 2312 | tf_op jit(solution)/shard_map/ppermute | solution.py:383
  33.1 3.5 %copy-start.8 = (s32[4]{0:T(128)S(1)}, s32[4]{0:T(128)}, u32[]{:S(2)}) copy-start(s32[4]{0:T(128)} %pad_add_fusion.where_ref) | copy-start | bytes 52
  37.9 2.1 %copy-start.10 = (f32[8,384]{1,0:T(8,128)}, f32[8,384]{1,0:T(8,128)S(1)}, u32[]{:S(2)}) copy-start(f32[8,384]{1,0:T(8,128)S(1)} %get-tuple-element.41.refs_5_) | copy-start | bytes 36868
  38.0 31.4 %copy-start.5 = (f32[384,128]{1,0:T(8,128)}, f32[384,128]{1,0:T(8,128)S(1)}, u32[]{:S(2)}) copy-start(f32[384,128]{1,0:T(8,128)S(1)} %get-tuple-element.34.refs_4_) | copy-start | bytes 589828
  40.0 29.4 %copy-start.1 = (bf16[384,2048]{1,0:T(8,128)(2,1)S(1)}, bf16[384,2048]{1,0:T(8,128)(2,1)}, u32[]{:S(2)}) copy-start(bf16[384,2048]{1,0:T(8,128)(2,1)} %shard_map.136.refs_0_) | copy-start | bytes 4718596
  40.0 29.4 %all-to-all-start.1 = ((bf16[8,256,256]{2,1,0:T(8,128)(2,1)}), bf16[8,256,256]{2,1,0:T(8,128)(2,1)S(1)}, u32[]{:S(2)}, u32[]{:S(2)}) async-start(bf16[8,256,256]{2,1,0:T(8,128)(2,1)} %broadcast_in_dim.4), calls=%async_computation.1 | async-start | bytes 2097152 | tf_op jit(solution)/shard_map/all_to_all | solution.py:37
  47.9 23.8 %copy-start.3 = (f32[384,128]{1,0:T(8,128)}, f32[384,128]{1,0:T(8,128)S(1)}, u32[]{:S(2)}) copy-start(f32[384,128]{1,0:T(8,128)S(1)} %get-tuple-element.54.refs_2_.refs_1_) | copy-start | bytes 589828
  48.0 23.7 %copy-start.4 = (f32[384,128]{1,0:T(8,128)}, f32[384,128]{1,0:T(8,128)S(1)}, u32[]{:S(2)}) copy-start(f32[384,128]{1,0:T(8,128)S(1)} %get-tuple-element.55.refs_3_.refs_2_) | copy-start | bytes 589828
  71.7 27.5 %copy-start.6 = (bf16[384,256]{1,0:T(8,128)(2,1)}, bf16[384,256]{1,0:T(8,128)(2,1)S(1)}, u32[]{:S(2)}) copy-start(bf16[384,256]{1,0:T(8,128)(2,1)S(1)} %get-tuple-element.40.refs_3_) | copy-start | bytes 589828
  71.7 14.9 %all-to-all-start.2 = ((bf16[8,144,128]{2,1,0:T(8,128)(2,1)}), bf16[8,144,128]{2,1,0:T(8,128)(2,1)S(1)}, u32[]{:S(2)}, u32[]{:S(2)}) async-start(bf16[8,144,128]{2,1,0:T(8,128)(2,1)} %get-tuple-element.35), calls=%async_computation.2 | async-start | bytes 589824 | tf_op jit(solution)/shard_map/all_to_all | solution.py:411
  76.1 9.1 %collective-permute-start.3 = (bf16[32,2048]{1,0:T(8,128)(2,1)S(1)}, bf16[32,2048]{1,0:T(8,128)(2,1)S(1)}, u32[]{:S(2)}, u32[]{:S(2)}) collective-permute-start(bf16[32,2048]{1,0:T(8,128)(2,1)S(1)} %slice_select_fusion), channel_id=1, source_target_pairs={{0,8},{4,12},{8,16},{12,20},{16,24},{20,28},{24,32},{28,36},{32,40... | collective-permute-start | bytes 393224 | tf_op jit(solution)/shard_map/ppermute | solution.py:410
  85.2 8.6 %copy-start.15 = (bf16[32,2048]{1,0:T(8,128)(2,1)}, bf16[32,2048]{1,0:T(8,128)(2,1)S(1)}, u32[]{:S(2)}) copy-start(bf16[32,2048]{1,0:T(8,128)(2,1)S(1)} %collective-permute-done.3.refs_1_) | copy-start | bytes 393220
  88.0 16.7 %all-to-all-start.3 = ((bf16[8,144,128]{2,1,0:T(8,128)(2,1)}), bf16[8,144,128]{2,1,0:T(8,128)(2,1)S(1)}, u32[]{:S(2)}, u32[]{:S(2)}) async-start(bf16[8,144,128]{2,1,0:T(8,128)(2,1)} %get-tuple-element.44), calls=%async_computation.3 | async-start | bytes 589824 | tf_op jit(solution)/shard_map/all_to_all | solution.py:420
  99.2 5.5 %copy-start.16 = (f32[8,2,384]{2,1,0:T(2,128)S(1)}, f32[8,2,384]{2,1,0:T(2,128)}, u32[]{:S(2)}) copy-start(f32[8,2,384]{2,1,0:T(2,128)} %get-tuple-element.48) | copy-start | bytes 73732
  99.2 17.3 %copy-start = (bf16[8,3,256,256]{3,2,1,0:T(8,128)(2,1)S(1)}, bf16[8,3,256,256]{3,2,1,0:T(8,128)(2,1)}, u32[]{:S(2)}) copy-start(bf16[8,3,256,256]{3,2,1,0:T(8,128)(2,1)} %all-gather.2.cloned.1.call-done.refs_4_.refs_7_.refs_6_) | copy-start | bytes 9437188
  99.2 17.2 %copy-start.9 = (s32[4]{0:T(128)S(1)}, s32[4]{0:T(128)}, u32[]{:S(2)}) copy-start(s32[4]{0:T(128)} %pad_add_fusion.where_ref) | copy-start | bytes 52
  99.2 17.2 %copy-start.12 = (f32[1024]{0:T(1024)S(1)}, f32[1024]{0:T(1024)}, u32[]{:S(2)}) copy-start(f32[1024]{0:T(1024)} %param.26) | copy-start | bytes 12292
  99.2 17.2 %copy-start.13 = (f32[1024]{0:T(1024)S(1)}, f32[1024]{0:T(1024)}, u32[]{:S(2)}) copy-start(f32[1024]{0:T(1024)} %param.25) | copy-start | bytes 12292
  116.5 1.2 copy-start.2
  119.8 4.2 %collective-permute-start.4 = (bf16[192,2048]{1,0:T(8,128)(2,1)S(1)}, bf16[192,2048]{1,0:T(8,128)(2,1)S(1)}, u32[]{:S(2)}, u32[]{:S(2)}) collective-permute-start(bf16[192,2048]{1,0:T(8,128)(2,1)S(1)} %get-tuple-element.50), channel_id=1, source_target_pairs={{0,4},{4,0},{1,5},{5,1},{2,6},{6,2},{3,7},{7,3},{8,12},{12,8},{9,1... | collective-permute-start | bytes 2359304 | tf_op jit(solution)/shard_map/ppermute | solution.py:452
Sparse Core Ops, SparseCore 0:
  39.1 48.1 all-gather.1
where the time goes:
time: 147 us; the launch traced here: 146 us
  starting transfers between devices  39.6 us (27%)
  waiting for transfers between devices  34.9 us (24%)
  blocking collectives  26.2 us (18%)
  Pallas kernels  24.1 us (16%)
  between operations  13.7 us (9%)
  local copies, waits for them, and re-layouts  4.28 us (3%)
  other arithmetic  3.61 us (2%)
    pallas_call x7, Pallas kernels, call(): pl.pallas_call(whole, out_shape=outs, in_specs=[pl.BlockSpec(memory_space...  21.7 us
    all_to_all x1, waiting for transfers between devices, told_to_all(): lax.all_to_all(copies, axis, 0, 0, axis_index_groups=groups, tiled=True)  21.4 us
    all_to_all x1, blocking collectives, per_device(): lax.all_to_all(partial.reshape(peers, rows // peers, width), 'tp', 0, 0,...  14.4 us
    all_to_all x1, blocking collectives, per_device(): stats = lax.all_to_all(stats, ('sp_2', 'tp'), 0, 0, tiled=True)  11.8 us
    ppermute x1, starting transfers between devices, per_device(): theirs = lax.ppermute(other, 'sp_2', swap)  8.75 us
    all_to_all x1, starting transfers between devices, told_to_all(): lax.all_to_all(copies, axis, 0, 0, axis_index_groups=groups, tiled=True)  6.95 us
    all_to_all x1, starting transfers between devices, per_device(): got = lax.all_to_all(sent, 'sp_0', 0, 0, tiled=True)  5.8 us
    ppermute x1, waiting for transfers between devices, per_device(): halo = lax.ppermute(last, SP, onward)  5.77 us
  transfers between devices with their start and end apart: 10, of which 6 were waited for; matrix products, arithmetic and copies ran while one was open for 2% of the time, Pallas kernels for 12%

commit v1 on v0

--- a/solution.py
+++ b/solution.py
@@ -125,6 +125,10 @@
     row_ref[...] = tall_dot(pick, col_ref[...], ((1,), (1,)))
 
 
+def hold(in_ref, out_ref):
+    out_ref[...] = in_ref[...]
+
+
 def spread(mine_ref, theirs_ref, out_ref):
     core = lax.axis_index("sp_2")
     height = mine_ref.shape[0]
@@ -263,7 +267,7 @@
         stats_ref[k, 1:2, :] = second[0:1]
 
 
-def inner_part(where_ref, normed_ref, cos_ref, sin_ref, key_value_ref, col_ref, row_ref, sums_ref, near_ref, packed_ref, qg_ref):
+def inner_part(where_ref, normed_ref, cos_ref, sin_ref, key_value_ref, col_ref, row_ref, near_ref, packed_ref, qg_ref):
     in_order(qg_ref, where_ref[2], near_ref)
     both = jnp.dot(normed_ref[...], qg_ref[...], preferred_element_type=F32)
     raw = both[:, :HEAD_DIM].astype(BF).astype(F32)
@@ -272,7 +276,6 @@
     packed_ref[:, HEAD_DIM : 2 * HEAD_DIM] = query.astype(F32)
     packed_ref[:, 2 * HEAD_DIM : 3 * HEAD_DIM] = gate * jax.nn.sigmoid(gate)
     packed_ref[:, 3 * HEAD_DIM : 4 * HEAD_DIM] = jnp.exp(col_ref[...])
-    packed_ref[:, 4 * HEAD_DIM :] = sums_ref[...]
     rows = query.shape[0]
     for at in range(0, rows, 128):
         upto = at + 128
@@ -284,6 +287,12 @@
         decay = jnp.where(seen, jnp.exp(jnp.where(seen, gap, 0.0)), 0.0)
         weight = (scores * decay).astype(BF)
         packed_ref[at:upto, :HEAD_DIM] = jnp.dot(weight, key_value_ref[0:upto, HEAD_DIM:], preferred_element_type=F32)
+
+
+def middle_part(where_ref, normed_ref, halo_ref, gain_ref, taps_ref, cos_ref, sin_ref, key_value_ref, col_ref, row_ref, near_ref, late_ref, stats_ref, packed_ref, w_ref, gated_ref, qg_ref):
+    sums_ref = packed_ref.at[:, 4 * HEAD_DIM : 5 * HEAD_DIM]
+    conv_part(where_ref, normed_ref, halo_ref, gain_ref, taps_ref, near_ref, sums_ref, stats_ref, w_ref, gated_ref)
+    inner_part(where_ref, normed_ref, cos_ref, sin_ref, key_value_ref, col_ref, row_ref, late_ref, packed_ref, qg_ref)
 
 
 def outer_part(where_ref, packed_ref, inside_ref, got_ref, gain_ref, stats_ref, conv_gain_ref, blocks_ref, keep_ref, send_ref, hidden_ref, out_ref):
@@ -357,7 +366,7 @@
 
     parts = (key_w, value_w, conv_value_w, conv_gate_w, query_w, out_gate_w, conv_out_w, ret_out_w)
     half = like((key_w.shape[0], 8 * HEAD_DIM), BF)
-    mine, other = pl.pallas_call(
+    own, other = pl.pallas_call(
         assemble,
         out_shape=[half, half],
         in_specs=[pl.BlockSpec(memory_space=pl.ANY) for _ in parts],
@@ -368,6 +377,15 @@
     )(*parts)
     swap = [(0, 1), (1, 0)]
     theirs = lax.ppermute(other, "sp_2", swap)
+    mine = pl.pallas_call(
+        hold,
+        out_shape=half,
+        in_specs=[pl.BlockSpec(memory_space=pltpu.VMEM)],
+        out_specs=pl.BlockSpec(memory_space=pltpu.VMEM),
+        compiler_params=pltpu.CompilerParams(vmem_limit_bytes=4 * 1024 * 1024),
+        name="hold",
+    )
+    mine = mine(own)
     copies = pl.pallas_call(
         spread,
         out_shape=like((RING, 2 * key_w.shape[0], 8 * HEAD_DIM), BF),
@@ -419,25 +437,19 @@
     )
     got = lax.all_to_all(sent, "sp_0", 0, 0, tiled=True)
 
-    sums, stats = call(
-        conv_part,
-        [like((both_rows, HEAD_DIM), F32), like((8, 2, both_rows), F32)],
+    stats, packed = call(
+        middle_part,
+        [like((8, 2, both_rows), F32), like((both_rows, 5 * HEAD_DIM), F32)],
         where,
-        (normed, halo, norm_gain.reshape(1, width), conv_taps, others),
-        [pltpu.VMEM((width, 2 * HEAD_DIM), BF), pltpu.VMEM((HALO + both_rows, HEAD_DIM), F32)],
-        far=(0, 1, 2),
-        parts=((4, 0),),
+        (normed, halo, norm_gain.reshape(1, width), conv_taps, cosine, sine, key_value_rows, col, row, others, others),
+        [
+            pltpu.VMEM((width, 2 * HEAD_DIM), BF),
+            pltpu.VMEM((HALO + both_rows, HEAD_DIM), F32),
+            pltpu.VMEM((width, 2 * HEAD_DIM), BF),
+        ],
+        far=(0, 1, 2, 4, 5, 6, 7, 8),
+        parts=((9, 0), (10, 1)),
         far_outs=(0, 1),
-    )
-    (packed,) = call(
-        inner_part,
-        [like((both_rows, 5 * HEAD_DIM), F32)],
-        where,
-        (normed, cosine, sine, key_value_rows, col, row, sums, others),
-        [pltpu.VMEM((width, 2 * HEAD_DIM), BF)],
-        far=(0, 1, 2, 3, 4, 5, 6),
-        parts=((7, 1),),
-        far_outs=(0,),
     )
     stats, packed, got = lax.optimization_barrier((stats, packed, got))
     stats = lax.all_to_all(stats, ("sp_2", "tp"), 0, 0, tiled=True)

time: 147 us -> 147 us (level)
  Pallas kernels: 24.1 us -> 21.6 us
    pallas_call x7 -> x6, Pallas kernels: 21.7 us -> 19.1 us  [call(): pl.pallas_call(whole, out_shape=outs, in_specs=[pl.BlockSpec(memory_space...]
    all_to_all x1, waiting for transfers between devices: 0.01 us -> 1.82 us  [per_device(): got = lax.all_to_all(sent, 'sp_0', 0, 0, tiled=True)]
  transfers between devices with their start and end apart: 10 -> 10, of which waited for: 6 -> 7; matrix products, arithmetic and copies ran while one was open for 2% -> 3% of each run, Pallas kernels for 12% -> 11%
where the time goes in v1:
time: 147 us; the launch traced here: 146 us
  starting transfers between devices  39.7 us (27%)
  waiting for transfers between devices  35.3 us (24%)
  blocking collectives  27.2 us (19%)
  Pallas kernels  21.6 us (15%)
  between operations  13.7 us (9%)
  local copies, waits for them, and re-layouts  4.88 us (3%)
  other arithmetic  3.68 us (3%)
    all_to_all x1, waiting for transfers between devices, told_to_all(): lax.all_to_all(copies, axis, 0, 0, axis_index_groups=groups, tiled=True)  21.6 us
    pallas_call x6, Pallas kernels, call(): pl.pallas_call(whole, out_shape=outs, in_specs=[pl.BlockSpec(memory_space...  19.1 us
    all_to_all x1, blocking collectives, per_device(): lax.all_to_all(partial.reshape(peers, rows // peers, width), 'tp', 0, 0,...  14.4 us
    all_to_all x1, blocking collectives, per_device(): stats = lax.all_to_all(stats, ('sp_2', 'tp'), 0, 0, tiled=True)  12.8 us
    ppermute x1, starting transfers between devices, per_device(): theirs = lax.ppermute(other, 'sp_2', swap)  8.75 us
    all_to_all x1, starting transfers between devices, told_to_all(): lax.all_to_all(copies, axis, 0, 0, axis_index_groups=groups, tiled=True)  6.95 us
    ppermute x1, waiting for transfers between devices, per_device(): halo = lax.ppermute(last, SP, onward)  6.06 us
    all_to_all x1, starting transfers between devices, per_device(): got = lax.all_to_all(sent, 'sp_0', 0, 0, tiled=True)  5.94 us
  transfers between devices with their start and end apart: 10, of which 7 were waited for; matrix products, arithmetic and copies ran while one was open for 3% of the time, Pallas kernels for 11%

profile of v1, /device:TPU:1, one launch (start us, length us, event | category | flops | bytes accessed | tf_op | source)
XLA Modules:
  0.0 146.0 jit_solution(10126073238970806190)
XLA Ops:
  6.5 1.6 %assemble.1 = (bf16[16,1024]{1,0:T(8,128)(2,1)}, bf16[16,1024]{1,0:T(8,128)(2,1)}) custom-call(bf16[16,256]{1,0:T(8,128)(2,1)} %refs_0_.3, bf16[16,256]{1,0:T(8,128)(2,1)} %refs_1_.1, bf16[16,256]{1,0:T(8,128)(2,1)} %refs_2_.1, bf16[16,256]{1,0:T(8,128)(2,1)} %refs_3_.2, bf16[16,256]{1,0:T(8,128)(2,1)} %refs_4_.1, bf16[16,256]{1,0:T(8,128)(2,1)} %refs_5_.1, ...), custom_call_target="tpu_custom_call" | custom-call | tf_op jit(solution)/shard_map/assemble/pallas_call | solution.py:369
  8.1 8.7 %collective-permute-start = (bf16[16,1024]{1,0:T(8,128)(2,1)}, bf16[16,1024]{1,0:T(8,128)(2,1)S(1)}, u32[]{:S(2)}, u32[]{:S(2)}) collective-permute-start(bf16[16,1024]{1,0:T(8,128)(2,1)} %get-tuple-element.29), channel_id=1, source_target_pairs={{0,4},{4,0},{1,5},{5,1},{2,6},{6,2},{3,7},{7,3},{8,12},{12,8},{9,1... | collective-permute-start | bytes 98312 | tf_op jit(solution)/shard_map/ppermute | solution.py:379
  16.9 0.0 copy-start.7
  16.9 0.7 copy-done.7
  17.7 0.3 collective-permute-done.theirs_ref
  17.9 0.8 spread.1
  18.8 4.7 %all-to-all-start = ((bf16[8,32,1024]{2,1,0:T(8,128)(2,1)}), bf16[8,32,1024]{2,1,0:T(8,128)(2,1)S(1)}, u32[]{:S(2)}, u32[]{:S(2)}) async-start(bf16[8,32,1024]{2,1,0:T(8,128)(2,1)} %spread.1), calls=%async_computation | async-start | bytes 1048576 | tf_op jit(solution)/shard_map/all_to_all | solution.py:397
  23.5 0.0 all-gather.2.cloned.1.call-start
  23.5 0.0 copy-done.14
  23.5 1.9 %collective-permute-start.2 = (bf16[192,2048]{1,0:T(8,128)(2,1)S(1)}, bf16[192,2048]{1,0:T(8,128)(2,1)}, u32[]{:S(2)}, u32[]{:S(2)}) collective-permute-start(bf16[192,2048]{1,0:T(8,128)(2,1)S(1)} %copy-done.14), channel_id=1, source_target_pairs={{0,4},{4,0},{1,5},{5,1},{2,6},{6,2},{3,7},{7,3},{8,12},{12,8},{9,1... | collective-permute-start | bytes 2359304 | tf_op jit(solution)/shard_map/ppermute | solution.py:400
  25.5 0.0 copy-done.11
  25.5 2.4 %collective-permute-start.1 = (f32[1,192]{1,0:T(1,128)S(1)}, f32[1,192]{1,0:T(1,128)S(1)}, u32[]{:S(2)}, u32[]{:S(2)}) collective-permute-start(f32[1,192]{1,0:T(1,128)S(1)} %constant_dynamic-slice_fusion), channel_id=1, source_target_pairs={{0,4},{4,0},{1,5},{5,1},{2,6},{6,2},{3,7},{7,3},{8,12},{12,8},{9,1... | collective-permute-start | bytes 2312 | tf_op jit(solution)/shard_map/ppermute | solution.py:401
  27.9 0.7 pad_add_fusion.where_ref
  28.6 0.0 collective-permute-done.2.refs_1_
  28.6 3.9 %shard_map.136.refs_0_ = bf16[384,2048]{1,0:T(8,128)(2,1)} custom-call(s32[4]{0:T(128)} %pad_add_fusion.where_ref, bf16[192,2048]{1,0:T(8,128)(2,1)} %refs_0_.4, bf16[192,2048]{1,0:T(8,128)(2,1)} %collective-permute-done.2.refs_1_, f32[1,2048]{1,0:T(1,128)} %bitcast.20), custom_call_target="tpu_custom_call" | custom-call | tf_op jit(solution)/shard_map/pallas_call | solution.py:74
  32.5 0.0 collective-permute-done.1.refs_1_
  32.5 3.1 %all-to-all-done = bf16[8,32,1024]{2,1,0:T(8,128)(2,1)S(1)} async-done(((bf16[8,32,1024]{2,1,0:T(8,128)(2,1)}), bf16[8,32,1024]{2,1,0:T(8,128)(2,1)S(1)}, u32[]{:S(2)}, u32[]{:S(2)}) %all-to-all-start) | async-done | bytes 524320 | tf_op jit(solution)/shard_map/all_to_all | solution.py:397
  35.6 0.0 copy-done.8
  35.6 1.3 shard_map.137
  36.9 0.2 copy.17
  37.2 0.9 copy.18
  38.1 0.0 all-gather.2.cloned.1.call-update
  38.2 0.0 copy-done.10
  38.2 1.0 broadcast_in_dim.4
  39.2 7.0 %all-to-all-start.1 = ((bf16[8,256,256]{2,1,0:T(8,128)(2,1)}), bf16[8,256,256]{2,1,0:T(8,128)(2,1)S(1)}, u32[]{:S(2)}, u32[]{:S(2)}) async-start(bf16[8,256,256]{2,1,0:T(8,128)(2,1)} %broadcast_in_dim.4), calls=%async_computation.1 | async-start | bytes 2097152 | tf_op jit(solution)/shard_map/all_to_all | solution.py:37
  46.2 0.8 fusion
  47.0 0.2 pad_maximum_fusion
  47.1 0.0 copy-start.2
  47.2 0.0 copy-start.3
  47.2 21.6 %all-to-all-done.1.refs_1_ = bf16[8,256,256]{2,1,0:T(8,128)(2,1)S(1)} async-done(((bf16[8,256,256]{2,1,0:T(8,128)(2,1)}), bf16[8,256,256]{2,1,0:T(8,128)(2,1)S(1)}, u32[]{:S(2)}, u32[]{:S(2)}) %all-to-all-start.1) | async-done | bytes 1048608 | tf_op jit(solution)/shard_map/all_to_all | solution.py:37
  68.7 0.0 copy-done.5
  68.7 0.0 copy-done.1
  68.7 2.3 %shard_map.138 = (bf16[384,256]{1,0:T(8,128)(2,1)S(1)}, bf16[8,144,128]{2,1,0:T(8,128)(2,1)}) custom-call(s32[4]{0:T(128)S(1)} %copy-done.8, bf16[384,2048]{1,0:T(8,128)(2,1)S(1)} %copy-done.1, bf16[8,256,256]{2,1,0:T(8,128)(2,1)S(1)} %all-to-all-done.1.refs_1_, f32[384,128]{1,0:T(8,128)S(1)} %get-tuple-element.54.refs_2_.refs_4_, ...), custom_call_target="tpu_custom_call" | custom-call | tf_op jit(solution)/shard_map/pallas_call | solution.py:74
  71.0 0.0 copy-done.2
  71.0 0.0 copy-done.3
  71.0 3.4 %all-to-all-start.2 = ((bf16[8,144,128]{2,1,0:T(8,128)(2,1)}), bf16[8,144,128]{2,1,0:T(8,128)(2,1)S(1)}, u32[]{:S(2)}, u32[]{:S(2)}) async-start(bf16[8,144,128]{2,1,0:T(8,128)(2,1)} %get-tuple-element.35), calls=%async_computation.2 | async-start | bytes 589824 | tf_op jit(solution)/shard_map/all_to_all | solution.py:429
  74.5 1.0 slice_select_fusion
  75.4 3.3 %collective-permute-start.3 = (bf16[32,2048]{1,0:T(8,128)(2,1)S(1)}, bf16[32,2048]{1,0:T(8,128)(2,1)S(1)}, u32[]{:S(2)}, u32[]{:S(2)}) collective-permute-start(bf16[32,2048]{1,0:T(8,128)(2,1)S(1)} %slice_select_fusion), channel_id=1, source_target_pairs={{0,8},{4,12},{8,16},{12,20},{16,24},{20,28},{24,32},{28,36},{32,40... | collective-permute-start | bytes 393224 | tf_op jit(solution)/shard_map/ppermute | solution.py:428
  78.7 6.1 %collective-permute-done.3.refs_1_ = bf16[32,2048]{1,0:T(8,128)(2,1)S(1)} collective-permute-done((bf16[32,2048]{1,0:T(8,128)(2,1)S(1)}, bf16[32,2048]{1,0:T(8,128)(2,1)S(1)}, u32[]{:S(2)}, u32[]{:S(2)}) %collective-permute-start.3) | collective-permute-done | bytes 131104 | tf_op jit(solution)/shard_map/ppermute | solution.py:428
  84.8 0.6 copy-done.15
  85.4 0.6 all-to-all-done.2.refs_0_
  86.0 1.3 shard_map.140
  87.4 5.9 %all-to-all-start.3 = ((bf16[8,144,128]{2,1,0:T(8,128)(2,1)}), bf16[8,144,128]{2,1,0:T(8,128)(2,1)S(1)}, u32[]{:S(2)}, u32[]{:S(2)}) async-start(bf16[8,144,128]{2,1,0:T(8,128)(2,1)} %get-tuple-element.44), calls=%async_computation.3 | async-start | bytes 589824 | tf_op jit(solution)/shard_map/all_to_all | solution.py:438
  93.3 0.0 all-gather.2.cloned.1.call-done.refs_9_.refs_10_.refs_6_
  93.3 0.0 copy-done.6
  93.4 0.0 copy-start
  93.4 0.0 copy-start.9
  93.4 0.0 copy-start.12
  93.4 0.0 copy-start.13
  93.4 8.1 %shard_map.139 = (f32[8,2,384]{2,1,0:T(2,128)}, f32[384,640]{1,0:T(8,128)}) custom-call(s32[4]{0:T(128)} %pad_add_fusion.where_ref, bf16[384,2048]{1,0:T(8,128)(2,1)} %shard_map.136.refs_0_, bf16[32,2048]{1,0:T(8,128)(2,1)} %copy-done.15, f32[1,2048]{1,0:T(1,128)} %bitcast.21, bf16[31,1024]{1,0:T(8,128)(2,1)} %refs_3_.3, f32[384,128]{1,0:T(8,128)} %copy-done.2, ...), custom_call_target="tpu_custom_call" | custom-call | tf_op jit(solution)/shard_map/pallas_call | solution.py:74
  101.5 1.8 %all-to-all-done.3.refs_2_ = bf16[8,144,128]{2,1,0:T(8,128)(2,1)S(1)} async-done(((bf16[8,144,128]{2,1,0:T(8,128)(2,1)}), bf16[8,144,128]{2,1,0:T(8,128)(2,1)S(1)}, u32[]{:S(2)}, u32[]{:S(2)}) %all-to-all-start.3) | async-done | bytes 294944 | tf_op jit(solution)/shard_map/all_to_all | solution.py:438
  103.4 12.8 %all_to_all.30.refs_4_ = f32[8,2,384]{2,1,0:T(2,128)S(1)} all-to-all(f32[8,2,384]{2,1,0:T(2,128)} %get-tuple-element.48), channel_id=1, replica_groups=mesh['sp_0'=8,'sp_1'=8,'sp_2'=2,'tp'=4] {'sp_2','tp'}, dimensions={0} | all-to-all | bytes 49152 | tf_op jit(solution)/shard_map/all_to_all | solution.py:455
  116.1 0.0 copy-done
  116.1 0.0 copy-done.9
  116.1 0.0 copy-done.12
  116.1 0.0 copy-done.13
  116.1 0.0 copy-start.4
  116.2 1.2 copy-done.4
  117.3 2.1 %shard_map.141 = (bf16[192,2048]{1,0:T(8,128)(2,1)S(1)}, bf16[192,2048]{1,0:T(8,128)(2,1)S(1)}) custom-call(s32[4]{0:T(128)S(1)} %copy-done.9, f32[384,640]{1,0:T(8,128)S(1)} %copy-done.4, f32[136,128]{1,0:T(8,128)S(1)} %get-tuple-element.46.refs_1_, bf16[8,144,128]{2,1,0:T(8,128)(2,1)S(1)} %all-to-all-done.3.refs_2_, f32[1,1024]{1,0:T(1,128)S(1)} %bitcast.14, ...), custom_call_target="tpu_custom_call" | custom-call | tf_op jit(solution)/shard_map/pallas_call | solution.py:74
  119.5 2.3 %collective-permute-start.4 = (bf16[192,2048]{1,0:T(8,128)(2,1)S(1)}, bf16[192,2048]{1,0:T(8,128)(2,1)S(1)}, u32[]{:S(2)}, u32[]{:S(2)}) collective-permute-start(bf16[192,2048]{1,0:T(8,128)(2,1)S(1)} %get-tuple-element.50), channel_id=1, source_target_pairs={{0,4},{4,0},{1,5},{5,1},{2,6},{6,2},{3,7},{7,3},{8,12},{12,8},{9,1... | collective-permute-start | bytes 2359304 | tf_op jit(solution)/shard_map/ppermute | solution.py:464
  121.8 1.9 %collective-permute-done.4 = bf16[192,2048]{1,0:T(8,128)(2,1)S(1)} collective-permute-done((bf16[192,2048]{1,0:T(8,128)(2,1)S(1)}, bf16[192,2048]{1,0:T(8,128)(2,1)S(1)}, u32[]{:S(2)}, u32[]{:S(2)}) %collective-permute-start.4) | collective-permute-done | bytes 786464 | tf_op jit(solution)/shard_map/ppermute | solution.py:464
  123.7 0.3 add_convert_fusion
  124.0 14.4 %all_to_all.31 = bf16[4,48,2048]{2,1,0:T(8,128)(2,1)S(1)} all-to-all(bf16[4,48,2048]{2,1,0:T(8,128)(2,1)S(1)} %bitcast.16), channel_id=1, replica_groups=mesh['sp_0'=8,'sp_1'=8,'sp_2'=2,'tp'=4] {'tp'}, dimensions={0} | all-to-all | bytes 1572864 | tf_op jit(solution)/shard_map/all_to_all | solution.py:467
  138.4 0.8 reduce_sum.12
  (14 shorter events, 0.1 us)
Async XLA Ops:
  6.5 18.9 %copy-start.11 = (f32[2,192]{1,0:T(2,128)S(1)}, f32[2,192]{1,0:T(2,128)}, u32[]{:S(2)}) copy-start(f32[2,192]{1,0:T(2,128)} %refs_0_.5) | copy-start | bytes 4612
  8.1 9.8 %collective-permute-start = (bf16[16,1024]{1,0:T(8,128)(2,1)}, bf16[16,1024]{1,0:T(8,128)(2,1)S(1)}, u32[]{:S(2)}, u32[]{:S(2)}) collective-permute-start(bf16[16,1024]{1,0:T(8,128)(2,1)} %get-tuple-element.29), channel_id=1, source_target_pairs={{0,4},{4,0},{1,5},{5,1},{2,6},{6,2},{3,7},{7,3},{8,12},{12,8},{9,1... | collective-permute-start | bytes 98312 | tf_op jit(solution)/shard_map/ppermute | solution.py:379
  16.9 0.8 copy-start.7
  17.7 5.9 %copy-start.14 = (bf16[192,2048]{1,0:T(8,128)(2,1)S(1)}, bf16[192,2048]{1,0:T(8,128)(2,1)}, u32[]{:S(2)}) copy-start(bf16[192,2048]{1,0:T(8,128)(2,1)} %refs_0_.4) | copy-start | bytes 2359300
  18.8 16.8 %all-to-all-start = ((bf16[8,32,1024]{2,1,0:T(8,128)(2,1)}), bf16[8,32,1024]{2,1,0:T(8,128)(2,1)S(1)}, u32[]{:S(2)}, u32[]{:S(2)}) async-start(bf16[8,32,1024]{2,1,0:T(8,128)(2,1)} %spread.1), calls=%async_computation | async-start | bytes 1048576 | tf_op jit(solution)/shard_map/all_to_all | solution.py:397
  23.5 69.9 %all-gather.2.cloned.1.call-start = ((), (), s32[]{:S(2)}) async-start(), calls=%async_computation.6 | async-start | bytes 3538944 | tf_op jit(solution)/shard_map/all_gather | solution.py:414
  23.5 5.0 %collective-permute-start.2 = (bf16[192,2048]{1,0:T(8,128)(2,1)S(1)}, bf16[192,2048]{1,0:T(8,128)(2,1)}, u32[]{:S(2)}, u32[]{:S(2)}) collective-permute-start(bf16[192,2048]{1,0:T(8,128)(2,1)S(1)} %copy-done.14), channel_id=1, source_target_pairs={{0,4},{4,0},{1,5},{5,1},{2,6},{6,2},{3,7},{7,3},{8,12},{12,8},{9,1... | collective-permute-start | bytes 2359304 | tf_op jit(solution)/shard_map/ppermute | solution.py:400
  25.5 7.0 %collective-permute-start.1 = (f32[1,192]{1,0:T(1,128)S(1)}, f32[1,192]{1,0:T(1,128)S(1)}, u32[]{:S(2)}, u32[]{:S(2)}) collective-permute-start(f32[1,192]{1,0:T(1,128)S(1)} %constant_dynamic-slice_fusion), channel_id=1, source_target_pairs={{0,4},{4,0},{1,5},{5,1},{2,6},{6,2},{3,7},{7,3},{8,12},{12,8},{9,1... | collective-permute-start | bytes 2312 | tf_op jit(solution)/shard_map/ppermute | solution.py:401
  28.6 7.1 %copy-start.8 = (s32[4]{0:T(128)S(1)}, s32[4]{0:T(128)}, u32[]{:S(2)}) copy-start(s32[4]{0:T(128)} %pad_add_fusion.where_ref) | copy-start | bytes 52
  36.9 1.2 copy-start.10
  36.9 31.8 %copy-start.5 = (f32[384,128]{1,0:T(8,128)}, f32[384,128]{1,0:T(8,128)S(1)}, u32[]{:S(2)}) copy-start(f32[384,128]{1,0:T(8,128)S(1)} %get-tuple-element.34.refs_4_.refs_7_) | copy-start | bytes 589828
  39.2 29.5 %copy-start.1 = (bf16[384,2048]{1,0:T(8,128)(2,1)S(1)}, bf16[384,2048]{1,0:T(8,128)(2,1)}, u32[]{:S(2)}) copy-start(bf16[384,2048]{1,0:T(8,128)(2,1)} %shard_map.136.refs_0_) | copy-start | bytes 4718596
  39.2 29.5 %all-to-all-start.1 = ((bf16[8,256,256]{2,1,0:T(8,128)(2,1)}), bf16[8,256,256]{2,1,0:T(8,128)(2,1)S(1)}, u32[]{:S(2)}, u32[]{:S(2)}) async-start(bf16[8,256,256]{2,1,0:T(8,128)(2,1)} %broadcast_in_dim.4), calls=%async_computation.1 | async-start | bytes 2097152 | tf_op jit(solution)/shard_map/all_to_all | solution.py:37
  47.1 23.9 %copy-start.2 = (f32[384,128]{1,0:T(8,128)}, f32[384,128]{1,0:T(8,128)S(1)}, u32[]{:S(2)}) copy-start(f32[384,128]{1,0:T(8,128)S(1)} %get-tuple-element.54.refs_2_.refs_4_) | copy-start | bytes 589828
  47.2 23.9 %copy-start.3 = (f32[384,128]{1,0:T(8,128)}, f32[384,128]{1,0:T(8,128)S(1)}, u32[]{:S(2)}) copy-start(f32[384,128]{1,0:T(8,128)S(1)} %get-tuple-element.55.refs_3_.refs_5_) | copy-start | bytes 589828
  71.0 22.3 %copy-start.6 = (bf16[384,256]{1,0:T(8,128)(2,1)}, bf16[384,256]{1,0:T(8,128)(2,1)S(1)}, u32[]{:S(2)}) copy-start(bf16[384,256]{1,0:T(8,128)(2,1)S(1)} %get-tuple-element.38.refs_6_) | copy-start | bytes 589828
  71.0 15.0 %all-to-all-start.2 = ((bf16[8,144,128]{2,1,0:T(8,128)(2,1)}), bf16[8,144,128]{2,1,0:T(8,128)(2,1)S(1)}, u32[]{:S(2)}, u32[]{:S(2)}) async-start(bf16[8,144,128]{2,1,0:T(8,128)(2,1)} %get-tuple-element.35), calls=%async_computation.2 | async-start | bytes 589824 | tf_op jit(solution)/shard_map/all_to_all | solution.py:429
  75.4 9.3 %collective-permute-start.3 = (bf16[32,2048]{1,0:T(8,128)(2,1)S(1)}, bf16[32,2048]{1,0:T(8,128)(2,1)S(1)}, u32[]{:S(2)}, u32[]{:S(2)}) collective-permute-start(bf16[32,2048]{1,0:T(8,128)(2,1)S(1)} %slice_select_fusion), channel_id=1, source_target_pairs={{0,8},{4,12},{8,16},{12,20},{16,24},{20,28},{24,32},{28,36},{32,40... | collective-permute-start | bytes 393224 | tf_op jit(solution)/shard_map/ppermute | solution.py:428
  84.8 0.6 copy-start.15
  87.4 16.0 %all-to-all-start.3 = ((bf16[8,144,128]{2,1,0:T(8,128)(2,1)}), bf16[8,144,128]{2,1,0:T(8,128)(2,1)S(1)}, u32[]{:S(2)}, u32[]{:S(2)}) async-start(bf16[8,144,128]{2,1,0:T(8,128)(2,1)} %get-tuple-element.44), calls=%async_computation.3 | async-start | bytes 589824 | tf_op jit(solution)/shard_map/all_to_all | solution.py:438
  93.4 22.8 %copy-start = (bf16[8,3,256,256]{3,2,1,0:T(8,128)(2,1)S(1)}, bf16[8,3,256,256]{3,2,1,0:T(8,128)(2,1)}, u32[]{:S(2)}) copy-start(bf16[8,3,256,256]{3,2,1,0:T(8,128)(2,1)} %all-gather.2.cloned.1.call-done.refs_9_.refs_10_.refs_6_) | copy-start | bytes 9437188
  93.4 22.8 %copy-start.9 = (s32[4]{0:T(128)S(1)}, s32[4]{0:T(128)}, u32[]{:S(2)}) copy-start(s32[4]{0:T(128)} %pad_add_fusion.where_ref) | copy-start | bytes 52
  93.4 22.8 %copy-start.12 = (f32[1024]{0:T(1024)S(1)}, f32[1024]{0:T(1024)}, u32[]{:S(2)}) copy-start(f32[1024]{0:T(1024)} %param.26) | copy-start | bytes 12292
  93.4 22.7 %copy-start.13 = (f32[1024]{0:T(1024)S(1)}, f32[1024]{0:T(1024)}, u32[]{:S(2)}) copy-start(f32[1024]{0:T(1024)} %param.25) | copy-start | bytes 12292
  116.1 1.2 copy-start.4
  119.5 4.2 %collective-permute-start.4 = (bf16[192,2048]{1,0:T(8,128)(2,1)S(1)}, bf16[192,2048]{1,0:T(8,128)(2,1)S(1)}, u32[]{:S(2)}, u32[]{:S(2)}) collective-permute-start(bf16[192,2048]{1,0:T(8,128)(2,1)S(1)} %get-tuple-element.50), channel_id=1, source_target_pairs={{0,4},{4,0},{1,5},{5,1},{2,6},{6,2},{3,7},{7,3},{8,12},{12,8},{9,1... | collective-permute-start | bytes 2359304 | tf_op jit(solution)/shard_map/ppermute | solution.py:464
Sparse Core Ops, SparseCore 0:
  38.3 47.7 all-gather.1

commit v2 on v1

--- a/solution.py
+++ b/solution.py
@@ -295,7 +295,7 @@
     inner_part(where_ref, normed_ref, cos_ref, sin_ref, key_value_ref, col_ref, row_ref, late_ref, packed_ref, qg_ref)
 
 
-def outer_part(where_ref, packed_ref, inside_ref, got_ref, gain_ref, stats_ref, conv_gain_ref, blocks_ref, keep_ref, send_ref, hidden_ref, out_ref):
+def outer_part(where_ref, packed_ref, inside_ref, got_ref, gain_ref, stats_ref, conv_gain_ref, blocks_ref, send_ref, own_ref, out_ref, hidden_ref):
     core = where_ref[2]
     here = where_ref[0]
     channel = pl.multiple_of((where_ref[3] * 2 + core) * HEAD_DIM, HEAD_DIM)
@@ -322,14 +322,19 @@
     chan_var = square - mean * mean
     v = (packed_ref[:, 4 * HEAD_DIM :] - mean) * lax.rsqrt(chan_var + EPSILON) * conv_gain_ref[:, pl.ds(channel, HEAD_DIM)]
     hidden_ref[:, :HEAD_DIM] = (v * jax.nn.sigmoid(v)).astype(BF)
-    half = keep_ref.shape[0]
+    half = send_ref.shape[0]
     for k in range(RING):
         set_rows(out_ref, core, k, blocks_ref[k, 2])
     mine = hidden_ref[pl.ds(pl.multiple_of(core * half, 64), half), :]
     theirs = hidden_ref[pl.ds(pl.multiple_of((1 - core) * half, 64), half), :]
     over_channels = (((1,), (1,)), ((), ()))
     send_ref[...] = lax.dot_general(theirs, out_ref[...], over_channels, preferred_element_type=F32).astype(BF)
-    keep_ref[...] = lax.dot_general(mine, out_ref[...], over_channels, preferred_element_type=F32).astype(BF)
+    own_ref[...] = mine
+
+
+def keep_part(own_ref, out_ref, keep_ref):
+    over_channels = (((1,), (1,)), ((), ()))
+    keep_ref[...] = lax.dot_general(own_ref[...], out_ref[...], over_channels, preferred_element_type=F32).astype(BF)
 
 
 def rotary_tables(start, count):
@@ -453,15 +458,23 @@
     )
     stats, packed, got = lax.optimization_barrier((stats, packed, got))
     stats = lax.all_to_all(stats, ("sp_2", "tp"), 0, 0, tiled=True)
-    keep, send = call(
+    send, own_rows, out_rows = call(
         outer_part,
-        [like((rows, width), BF), like((rows, width), BF)],
+        [like((rows, width), BF), like((rows, 2 * HEAD_DIM), BF), like((width, 2 * HEAD_DIM), BF)],
         where,
         (packed, inside, got, ret_gain.reshape(1, -1), stats, conv_gain.reshape(1, -1), others),
-        [pltpu.VMEM((both_rows, 2 * HEAD_DIM), BF), pltpu.VMEM((width, 2 * HEAD_DIM), BF)],
+        [pltpu.VMEM((both_rows, 2 * HEAD_DIM), BF)],
         mib=14,
     )
     other = lax.ppermute(send, "sp_2", swap)
+    keep = pl.pallas_call(
+        keep_part,
+        out_shape=like((rows, width), BF),
+        in_specs=[pl.BlockSpec(memory_space=pltpu.VMEM)] * 2,
+        out_specs=pl.BlockSpec(memory_space=pltpu.VMEM),
+        compiler_params=pltpu.CompilerParams(vmem_limit_bytes=8 * 1024 * 1024),
+        name="keep_part",
+    )(own_rows, out_rows)
     partial = (keep.astype(F32) + other.astype(F32)).astype(BF)
     peers = lax.axis_size("tp")
     arrived = lax.all_to_all(partial.reshape(peers, rows // peers, width), "tp", 0, 0, tiled=True)

time: 147 us -> 147 us (level)
  no operation moved by 1% of the time
where the time goes in v2:
time: 147 us; the launch traced here: 146 us
  starting transfers between devices  39.7 us (27%)
  waiting for transfers between devices  34.8 us (24%)
  blocking collectives  27.2 us (19%)
  Pallas kernels  21.7 us (15%)
  between operations  13.7 us (9%)
  local copies, waits for them, and re-layouts  4.88 us (3%)
  other arithmetic  3.68 us (3%)
    all_to_all x1, waiting for transfers between devices, told_to_all(): lax.all_to_all(copies, axis, 0, 0, axis_index_groups=groups, tiled=True)  21.6 us
    pallas_call x6, Pallas kernels, call(): pl.pallas_call(whole, out_shape=outs, in_specs=[pl.BlockSpec(memory_space...  18.8 us
    all_to_all x1, blocking collectives, per_device(): lax.all_to_all(partial.reshape(peers, rows // peers, width), 'tp', 0, 0,...  14.4 us
    all_to_all x1, blocking collectives, per_device(): stats = lax.all_to_all(stats, ('sp_2', 'tp'), 0, 0, tiled=True)  12.8 us
    ppermute x1, starting transfers between devices, per_device(): theirs = lax.ppermute(other, 'sp_2', swap)  8.75 us
    all_to_all x1, starting transfers between devices, told_to_all(): lax.all_to_all(copies, axis, 0, 0, axis_index_groups=groups, tiled=True)  6.95 us
    ppermute x1, waiting for transfers between devices, per_device(): halo = lax.ppermute(last, SP, onward)  6.06 us
    all_to_all x1, starting transfers between devices, per_device(): got = lax.all_to_all(sent, 'sp_0', 0, 0, tiled=True)  5.94 us
  transfers between devices with their start and end apart: 10, of which 7 were waited for; matrix products, arithmetic and copies ran while one was open for 3% of the time, Pallas kernels for 11%

profile of v2, /device:TPU:1, one launch (start us, length us, event | category | flops | bytes accessed | tf_op | source)
XLA Modules:
  0.0 145.7 jit_solution(15741763161245251275)
XLA Ops:
  6.5 1.6 %assemble.1 = (bf16[16,1024]{1,0:T(8,128)(2,1)}, bf16[16,1024]{1,0:T(8,128)(2,1)}) custom-call(bf16[16,256]{1,0:T(8,128)(2,1)} %refs_0_.3, bf16[16,256]{1,0:T(8,128)(2,1)} %refs_1_.1, bf16[16,256]{1,0:T(8,128)(2,1)} %refs_2_.1, bf16[16,256]{1,0:T(8,128)(2,1)} %refs_3_.2, bf16[16,256]{1,0:T(8,128)(2,1)} %refs_4_.1, bf16[16,256]{1,0:T(8,128)(2,1)} %refs_5_.1, ...), custom_call_target="tpu_custom_call" | custom-call | tf_op jit(solution)/shard_map/assemble/pallas_call | solution.py:374
  8.1 8.7 %collective-permute-start = (bf16[16,1024]{1,0:T(8,128)(2,1)}, bf16[16,1024]{1,0:T(8,128)(2,1)S(1)}, u32[]{:S(2)}, u32[]{:S(2)}) collective-permute-start(bf16[16,1024]{1,0:T(8,128)(2,1)} %get-tuple-element.30), channel_id=1, source_target_pairs={{0,4},{4,0},{1,5},{5,1},{2,6},{6,2},{3,7},{7,3},{8,12},{12,8},{9,1... | collective-permute-start | bytes 98312 | tf_op jit(solution)/shard_map/ppermute | solution.py:384
  16.9 0.0 copy-start.7
  16.9 0.7 copy-done.7
  17.7 0.3 collective-permute-done.theirs_ref
  17.9 0.8 spread.1
  18.8 4.7 %all-to-all-start = ((bf16[8,32,1024]{2,1,0:T(8,128)(2,1)}), bf16[8,32,1024]{2,1,0:T(8,128)(2,1)S(1)}, u32[]{:S(2)}, u32[]{:S(2)}) async-start(bf16[8,32,1024]{2,1,0:T(8,128)(2,1)} %spread.1), calls=%async_computation | async-start | bytes 1048576 | tf_op jit(solution)/shard_map/all_to_all | solution.py:402
  23.5 0.0 all-gather.2.cloned.1.call-start
  23.5 0.0 copy-done.14
  23.5 1.9 %collective-permute-start.2 = (bf16[192,2048]{1,0:T(8,128)(2,1)S(1)}, bf16[192,2048]{1,0:T(8,128)(2,1)}, u32[]{:S(2)}, u32[]{:S(2)}) collective-permute-start(bf16[192,2048]{1,0:T(8,128)(2,1)S(1)} %copy-done.14), channel_id=1, source_target_pairs={{0,4},{4,0},{1,5},{5,1},{2,6},{6,2},{3,7},{7,3},{8,12},{12,8},{9,1... | collective-permute-start | bytes 2359304 | tf_op jit(solution)/shard_map/ppermute | solution.py:405
  25.5 0.0 copy-done.11
  25.5 2.4 %collective-permute-start.1 = (f32[1,192]{1,0:T(1,128)S(1)}, f32[1,192]{1,0:T(1,128)S(1)}, u32[]{:S(2)}, u32[]{:S(2)}) collective-permute-start(f32[1,192]{1,0:T(1,128)S(1)} %constant_dynamic-slice_fusion), channel_id=1, source_target_pairs={{0,4},{4,0},{1,5},{5,1},{2,6},{6,2},{3,7},{7,3},{8,12},{12,8},{9,1... | collective-permute-start | bytes 2312 | tf_op jit(solution)/shard_map/ppermute | solution.py:406
  27.9 0.7 pad_add_fusion.where_ref
  28.6 0.0 collective-permute-done.2.refs_1_
  28.6 3.9 %shard_map.136.refs_0_ = bf16[384,2048]{1,0:T(8,128)(2,1)} custom-call(s32[4]{0:T(128)} %pad_add_fusion.where_ref, bf16[192,2048]{1,0:T(8,128)(2,1)} %refs_0_.4, bf16[192,2048]{1,0:T(8,128)(2,1)} %collective-permute-done.2.refs_1_, f32[1,2048]{1,0:T(1,128)} %bitcast.20), custom_call_target="tpu_custom_call" | custom-call | tf_op jit(solution)/shard_map/pallas_call | solution.py:74
  32.5 0.0 collective-permute-done.1.refs_1_
  32.5 3.1 %all-to-all-done = bf16[8,32,1024]{2,1,0:T(8,128)(2,1)S(1)} async-done(((bf16[8,32,1024]{2,1,0:T(8,128)(2,1)}), bf16[8,32,1024]{2,1,0:T(8,128)(2,1)S(1)}, u32[]{:S(2)}, u32[]{:S(2)}) %all-to-all-start) | async-done | bytes 524320 | tf_op jit(solution)/shard_map/all_to_all | solution.py:402
  35.6 0.0 copy-done.8
  35.6 1.3 shard_map.137
  36.9 0.2 copy.17
  37.2 0.9 copy.18
  38.1 0.0 all-gather.2.cloned.1.call-update
  38.2 0.0 copy-done.10
  38.2 1.0 broadcast_in_dim.4
  39.2 7.0 %all-to-all-start.1 = ((bf16[8,256,256]{2,1,0:T(8,128)(2,1)}), bf16[8,256,256]{2,1,0:T(8,128)(2,1)S(1)}, u32[]{:S(2)}, u32[]{:S(2)}) async-start(bf16[8,256,256]{2,1,0:T(8,128)(2,1)} %broadcast_in_dim.4), calls=%async_computation.1 | async-start | bytes 2097152 | tf_op jit(solution)/shard_map/all_to_all | solution.py:37
  46.2 0.8 fusion
  47.0 0.2 pad_maximum_fusion
  47.1 0.0 copy-start.2
  47.2 0.0 copy-start.3
  47.2 21.6 %all-to-all-done.1.refs_1_ = bf16[8,256,256]{2,1,0:T(8,128)(2,1)S(1)} async-done(((bf16[8,256,256]{2,1,0:T(8,128)(2,1)}), bf16[8,256,256]{2,1,0:T(8,128)(2,1)S(1)}, u32[]{:S(2)}, u32[]{:S(2)}) %all-to-all-start.1) | async-done | bytes 1048608 | tf_op jit(solution)/shard_map/all_to_all | solution.py:37
  68.7 0.0 copy-done.5
  68.7 0.0 copy-done.1
  68.7 2.3 %shard_map.138 = (bf16[384,256]{1,0:T(8,128)(2,1)S(1)}, bf16[8,144,128]{2,1,0:T(8,128)(2,1)}) custom-call(s32[4]{0:T(128)S(1)} %copy-done.8, bf16[384,2048]{1,0:T(8,128)(2,1)S(1)} %copy-done.1, bf16[8,256,256]{2,1,0:T(8,128)(2,1)S(1)} %all-to-all-done.1.refs_1_, f32[384,128]{1,0:T(8,128)S(1)} %get-tuple-element.56.refs_2_.refs_4_, ...), custom_call_target="tpu_custom_call" | custom-call | tf_op jit(solution)/shard_map/pallas_call | solution.py:74
  71.0 0.0 copy-done.2
  71.0 0.0 copy-done.3
  71.0 3.4 %all-to-all-start.2 = ((bf16[8,144,128]{2,1,0:T(8,128)(2,1)}), bf16[8,144,128]{2,1,0:T(8,128)(2,1)S(1)}, u32[]{:S(2)}, u32[]{:S(2)}) async-start(bf16[8,144,128]{2,1,0:T(8,128)(2,1)} %get-tuple-element.36), calls=%async_computation.2 | async-start | bytes 589824 | tf_op jit(solution)/shard_map/all_to_all | solution.py:434
  74.5 1.0 slice_select_fusion
  75.4 3.3 %collective-permute-start.3 = (bf16[32,2048]{1,0:T(8,128)(2,1)S(1)}, bf16[32,2048]{1,0:T(8,128)(2,1)S(1)}, u32[]{:S(2)}, u32[]{:S(2)}) collective-permute-start(bf16[32,2048]{1,0:T(8,128)(2,1)S(1)} %slice_select_fusion), channel_id=1, source_target_pairs={{0,8},{4,12},{8,16},{12,20},{16,24},{20,28},{24,32},{28,36},{32,40... | collective-permute-start | bytes 393224 | tf_op jit(solution)/shard_map/ppermute | solution.py:433
  78.7 6.1 %collective-permute-done.3.refs_1_ = bf16[32,2048]{1,0:T(8,128)(2,1)S(1)} collective-permute-done((bf16[32,2048]{1,0:T(8,128)(2,1)S(1)}, bf16[32,2048]{1,0:T(8,128)(2,1)S(1)}, u32[]{:S(2)}, u32[]{:S(2)}) %collective-permute-start.3) | collective-permute-done | bytes 131104 | tf_op jit(solution)/shard_map/ppermute | solution.py:433
  84.8 0.6 copy-done.15
  85.4 0.6 all-to-all-done.2.refs_0_
  86.0 1.3 shard_map.140
  87.4 5.9 %all-to-all-start.3 = ((bf16[8,144,128]{2,1,0:T(8,128)(2,1)}), bf16[8,144,128]{2,1,0:T(8,128)(2,1)S(1)}, u32[]{:S(2)}, u32[]{:S(2)}) async-start(bf16[8,144,128]{2,1,0:T(8,128)(2,1)} %get-tuple-element.45), calls=%async_computation.3 | async-start | bytes 589824 | tf_op jit(solution)/shard_map/all_to_all | solution.py:443
  93.3 0.0 all-gather.2.cloned.1.call-done.refs_9_.refs_10_.refs_6_
  93.3 0.0 copy-done.6
  93.4 0.0 copy-start
  93.4 0.0 copy-start.9
  93.4 0.0 copy-start.12
  93.4 0.0 copy-start.13
  93.4 8.1 %shard_map.139 = (f32[8,2,384]{2,1,0:T(2,128)}, f32[384,640]{1,0:T(8,128)}) custom-call(s32[4]{0:T(128)} %pad_add_fusion.where_ref, bf16[384,2048]{1,0:T(8,128)(2,1)} %shard_map.136.refs_0_, bf16[32,2048]{1,0:T(8,128)(2,1)} %copy-done.15, f32[1,2048]{1,0:T(1,128)} %bitcast.21, bf16[31,1024]{1,0:T(8,128)(2,1)} %refs_3_.3, f32[384,128]{1,0:T(8,128)} %copy-done.2, ...), custom_call_target="tpu_custom_call" | custom-call | tf_op jit(solution)/shard_map/pallas_call | solution.py:74
  101.5 1.8 %all-to-all-done.3.refs_2_ = bf16[8,144,128]{2,1,0:T(8,128)(2,1)S(1)} async-done(((bf16[8,144,128]{2,1,0:T(8,128)(2,1)}), bf16[8,144,128]{2,1,0:T(8,128)(2,1)S(1)}, u32[]{:S(2)}, u32[]{:S(2)}) %all-to-all-start.3) | async-done | bytes 294944 | tf_op jit(solution)/shard_map/all_to_all | solution.py:443
  103.4 12.8 %all_to_all.30.refs_4_ = f32[8,2,384]{2,1,0:T(2,128)S(1)} all-to-all(f32[8,2,384]{2,1,0:T(2,128)} %get-tuple-element.49), channel_id=1, replica_groups=mesh['sp_0'=8,'sp_1'=8,'sp_2'=2,'tp'=4] {'sp_2','tp'}, dimensions={0} | all-to-all | bytes 49152 | tf_op jit(solution)/shard_map/all_to_all | solution.py:460
  116.1 0.0 copy-done
  116.1 0.0 copy-done.9
  116.1 0.0 copy-done.12
  116.1 0.0 copy-done.13
  116.2 1.2 copy-done.4
  117.3 1.8 %shard_map.141 = (bf16[192,2048]{1,0:T(8,128)(2,1)S(1)}, bf16[192,256]{1,0:T(8,128)(2,1)S(1)}, bf16[2048,256]{1,0:T(8,128)(2,1)S(1)}) custom-call(s32[4]{0:T(128)S(1)} %copy-done.9, f32[384,640]{1,0:T(8,128)S(1)} %copy-done.4, f32[136,128]{1,0:T(8,128)S(1)} %get-tuple-element.47.refs_1_, bf16[8,144,128]{2,1,0:T(8,128)(2,1)S(1)} %all-to-all-done.3.refs_2_, ...), custom_call_target="tpu_custom_call" | custom-call | tf_op jit(solution)/shard_map/pallas_call | solution.py:74
  119.2 2.3 %collective-permute-start.4 = (bf16[192,2048]{1,0:T(8,128)(2,1)S(1)}, bf16[192,2048]{1,0:T(8,128)(2,1)S(1)}, u32[]{:S(2)}, u32[]{:S(2)}) collective-permute-start(bf16[192,2048]{1,0:T(8,128)(2,1)S(1)} %get-tuple-element.52), channel_id=1, source_target_pairs={{0,4},{4,0},{1,5},{5,1},{2,6},{6,2},{3,7},{7,3},{8,12},{12,8},{9,1... | collective-permute-start | bytes 2359304 | tf_op jit(solution)/shard_map/ppermute | solution.py:469
  121.5 0.5 keep_part.1
  122.0 1.4 collective-permute-done.4
  123.3 0.3 add_convert_fusion
  123.6 14.4 %all_to_all.31 = bf16[4,48,2048]{2,1,0:T(8,128)(2,1)S(1)} all-to-all(bf16[4,48,2048]{2,1,0:T(8,128)(2,1)S(1)} %bitcast.16), channel_id=1, replica_groups=mesh['sp_0'=8,'sp_1'=8,'sp_2'=2,'tp'=4] {'tp'}, dimensions={0} | all-to-all | bytes 1572864 | tf_op jit(solution)/shard_map/all_to_all | solution.py:480
  138.0 0.8 reduce_sum.12
  (15 shorter events, 0.1 us)
Async XLA Ops:
  6.5 18.9 %copy-start.11 = (f32[2,192]{1,0:T(2,128)S(1)}, f32[2,192]{1,0:T(2,128)}, u32[]{:S(2)}) copy-start(f32[2,192]{1,0:T(2,128)} %refs_0_.5) | copy-start | bytes 4612
  8.1 9.8 %collective-permute-start = (bf16[16,1024]{1,0:T(8,128)(2,1)}, bf16[16,1024]{1,0:T(8,128)(2,1)S(1)}, u32[]{:S(2)}, u32[]{:S(2)}) collective-permute-start(bf16[16,1024]{1,0:T(8,128)(2,1)} %get-tuple-element.30), channel_id=1, source_target_pairs={{0,4},{4,0},{1,5},{5,1},{2,6},{6,2},{3,7},{7,3},{8,12},{12,8},{9,1... | collective-permute-start | bytes 98312 | tf_op jit(solution)/shard_map/ppermute | solution.py:384
  16.9 0.8 copy-start.7
  17.7 5.9 %copy-start.14 = (bf16[192,2048]{1,0:T(8,128)(2,1)S(1)}, bf16[192,2048]{1,0:T(8,128)(2,1)}, u32[]{:S(2)}) copy-start(bf16[192,2048]{1,0:T(8,128)(2,1)} %refs_0_.4) | copy-start | bytes 2359300
  18.8 16.8 %all-to-all-start = ((bf16[8,32,1024]{2,1,0:T(8,128)(2,1)}), bf16[8,32,1024]{2,1,0:T(8,128)(2,1)S(1)}, u32[]{:S(2)}, u32[]{:S(2)}) async-start(bf16[8,32,1024]{2,1,0:T(8,128)(2,1)} %spread.1), calls=%async_computation | async-start | bytes 1048576 | tf_op jit(solution)/shard_map/all_to_all | solution.py:402
  23.5 69.9 %all-gather.2.cloned.1.call-start = ((), (), s32[]{:S(2)}) async-start(), calls=%async_computation.6 | async-start | bytes 3538944 | tf_op jit(solution)/shard_map/all_gather | solution.py:419
  23.5 5.0 %collective-permute-start.2 = (bf16[192,2048]{1,0:T(8,128)(2,1)S(1)}, bf16[192,2048]{1,0:T(8,128)(2,1)}, u32[]{:S(2)}, u32[]{:S(2)}) collective-permute-start(bf16[192,2048]{1,0:T(8,128)(2,1)S(1)} %copy-done.14), channel_id=1, source_target_pairs={{0,4},{4,0},{1,5},{5,1},{2,6},{6,2},{3,7},{7,3},{8,12},{12,8},{9,1... | collective-permute-start | bytes 2359304 | tf_op jit(solution)/shard_map/ppermute | solution.py:405
  25.5 7.0 %collective-permute-start.1 = (f32[1,192]{1,0:T(1,128)S(1)}, f32[1,192]{1,0:T(1,128)S(1)}, u32[]{:S(2)}, u32[]{:S(2)}) collective-permute-start(f32[1,192]{1,0:T(1,128)S(1)} %constant_dynamic-slice_fusion), channel_id=1, source_target_pairs={{0,4},{4,0},{1,5},{5,1},{2,6},{6,2},{3,7},{7,3},{8,12},{12,8},{9,1... | collective-permute-start | bytes 2312 | tf_op jit(solution)/shard_map/ppermute | solution.py:406
  28.6 7.1 %copy-start.8 = (s32[4]{0:T(128)S(1)}, s32[4]{0:T(128)}, u32[]{:S(2)}) copy-start(s32[4]{0:T(128)} %pad_add_fusion.where_ref) | copy-start | bytes 52
  36.9 1.2 copy-start.10
  36.9 31.8 %copy-start.5 = (f32[384,128]{1,0:T(8,128)}, f32[384,128]{1,0:T(8,128)S(1)}, u32[]{:S(2)}) copy-start(f32[384,128]{1,0:T(8,128)S(1)} %get-tuple-element.35.refs_4_.refs_7_) | copy-start | bytes 589828
  39.2 29.5 %copy-start.1 = (bf16[384,2048]{1,0:T(8,128)(2,1)S(1)}, bf16[384,2048]{1,0:T(8,128)(2,1)}, u32[]{:S(2)}) copy-start(bf16[384,2048]{1,0:T(8,128)(2,1)} %shard_map.136.refs_0_) | copy-start | bytes 4718596
  39.2 29.5 %all-to-all-start.1 = ((bf16[8,256,256]{2,1,0:T(8,128)(2,1)}), bf16[8,256,256]{2,1,0:T(8,128)(2,1)S(1)}, u32[]{:S(2)}, u32[]{:S(2)}) async-start(bf16[8,256,256]{2,1,0:T(8,128)(2,1)} %broadcast_in_dim.4), calls=%async_computation.1 | async-start | bytes 2097152 | tf_op jit(solution)/shard_map/all_to_all | solution.py:37
  47.1 23.9 %copy-start.2 = (f32[384,128]{1,0:T(8,128)}, f32[384,128]{1,0:T(8,128)S(1)}, u32[]{:S(2)}) copy-start(f32[384,128]{1,0:T(8,128)S(1)} %get-tuple-element.56.refs_2_.refs_4_) | copy-start | bytes 589828
  47.2 23.9 %copy-start.3 = (f32[384,128]{1,0:T(8,128)}, f32[384,128]{1,0:T(8,128)S(1)}, u32[]{:S(2)}) copy-start(f32[384,128]{1,0:T(8,128)S(1)} %get-tuple-element.57.refs_3_.refs_5_) | copy-start | bytes 589828
  71.0 22.3 %copy-start.6 = (bf16[384,256]{1,0:T(8,128)(2,1)}, bf16[384,256]{1,0:T(8,128)(2,1)S(1)}, u32[]{:S(2)}) copy-start(bf16[384,256]{1,0:T(8,128)(2,1)S(1)} %get-tuple-element.39.refs_6_) | copy-start | bytes 589828
  71.0 15.0 %all-to-all-start.2 = ((bf16[8,144,128]{2,1,0:T(8,128)(2,1)}), bf16[8,144,128]{2,1,0:T(8,128)(2,1)S(1)}, u32[]{:S(2)}, u32[]{:S(2)}) async-start(bf16[8,144,128]{2,1,0:T(8,128)(2,1)} %get-tuple-element.36), calls=%async_computation.2 | async-start | bytes 589824 | tf_op jit(solution)/shard_map/all_to_all | solution.py:434
  75.4 9.3 %collective-permute-start.3 = (bf16[32,2048]{1,0:T(8,128)(2,1)S(1)}, bf16[32,2048]{1,0:T(8,128)(2,1)S(1)}, u32[]{:S(2)}, u32[]{:S(2)}) collective-permute-start(bf16[32,2048]{1,0:T(8,128)(2,1)S(1)} %slice_select_fusion), channel_id=1, source_target_pairs={{0,8},{4,12},{8,16},{12,20},{16,24},{20,28},{24,32},{28,36},{32,40... | collective-permute-start | bytes 393224 | tf_op jit(solution)/shard_map/ppermute | solution.py:433
  84.8 0.6 copy-start.15
  87.4 16.0 %all-to-all-start.3 = ((bf16[8,144,128]{2,1,0:T(8,128)(2,1)}), bf16[8,144,128]{2,1,0:T(8,128)(2,1)S(1)}, u32[]{:S(2)}, u32[]{:S(2)}) async-start(bf16[8,144,128]{2,1,0:T(8,128)(2,1)} %get-tuple-element.45), calls=%async_computation.3 | async-start | bytes 589824 | tf_op jit(solution)/shard_map/all_to_all | solution.py:443
  93.4 22.8 %copy-start = (bf16[8,3,256,256]{3,2,1,0:T(8,128)(2,1)S(1)}, bf16[8,3,256,256]{3,2,1,0:T(8,128)(2,1)}, u32[]{:S(2)}) copy-start(bf16[8,3,256,256]{3,2,1,0:T(8,128)(2,1)} %all-gather.2.cloned.1.call-done.refs_9_.refs_10_.refs_6_) | copy-start | bytes 9437188
  93.4 22.8 %copy-start.9 = (s32[4]{0:T(128)S(1)}, s32[4]{0:T(128)}, u32[]{:S(2)}) copy-start(s32[4]{0:T(128)} %pad_add_fusion.where_ref) | copy-start | bytes 52
  93.4 22.8 %copy-start.12 = (f32[1024]{0:T(1024)S(1)}, f32[1024]{0:T(1024)}, u32[]{:S(2)}) copy-start(f32[1024]{0:T(1024)} %param.26) | copy-start | bytes 12292
  93.4 22.7 %copy-start.13 = (f32[1024]{0:T(1024)S(1)}, f32[1024]{0:T(1024)}, u32[]{:S(2)}) copy-start(f32[1024]{0:T(1024)} %param.25) | copy-start | bytes 12292
  116.1 1.2 copy-start.4
  119.2 4.2 %collective-permute-start.4 = (bf16[192,2048]{1,0:T(8,128)(2,1)S(1)}, bf16[192,2048]{1,0:T(8,128)(2,1)S(1)}, u32[]{:S(2)}, u32[]{:S(2)}) collective-permute-start(bf16[192,2048]{1,0:T(8,128)(2,1)S(1)} %get-tuple-element.52), channel_id=1, source_target_pairs={{0,4},{4,0},{1,5},{5,1},{2,6},{6,2},{3,7},{7,3},{8,12},{12,8},{9,1... | collective-permute-start | bytes 2359304 | tf_op jit(solution)/shard_map/ppermute | solution.py:469
Sparse Core Ops, SparseCore 0:
  38.3 47.7 all-gather.1
